TPU v7x, 128 devices: a whole 4x4x4 slice. The times are simulated.
128 devices in a mesh: sp: 16 (over z, y), tp: 4 (over x), dp: 2 (over core).
Axes of the slice: x: 4, y: 4, z: 4, core: 2. Of those that a mesh axis runs over, the one named last changes fastest.
Arguments:
- latent: bfloat16 [2, 12288, 2048], P('dp', ('sp', 'tp')), may hold values from -3 to 3
- cond: bfloat16 [2, 2048], P('dp', 'sp'), may hold values from -6 to 6
- cond_ctx: bfloat16 [2048], P('sp'), may hold values from -6 to 6
- context: bfloat16 [2, 512, 2048], P('dp', 'sp'), may hold values from -6 to 6
- norm_gain: bfloat16 [2048], replicated, may hold values from 0.099609375 to 1.8984375
- mod_shift: bfloat16 [2048, 2048], P('sp', 'tp'), may hold values from -0.125 to 0.125
- mod_scale: bfloat16 [2048, 2048], P('sp', 'tp'), may hold values from -0.125 to 0.125
- mod_gate: bfloat16 [2048, 2048], P('sp', 'tp'), may hold values from -0.125 to 0.125
- w_query: bfloat16 [2048, 1024], P(None, 'tp'), may hold values from -0.125 to 0.125
- w_key: bfloat16 [2048, 256], P(None, 'tp'), may hold values from -0.125 to 0.125
- w_value: bfloat16 [2048, 256], P(None, 'tp'), may hold values from -0.125 to 0.125
- q_gain: bfloat16 [64], replicated, may hold values from 1 to 5.5
- k_gain: bfloat16 [64], replicated, may hold values from 1 to 5.5
- ctx_lift: float32 [16], P('tp'), may hold values from 1 to 3
- w_out: bfloat16 [1024, 2048], replicated, may hold values from -1.5 to 1.5
Outputs:
- mixed: bfloat16 [2, 12288, 2048], P('dp', ('sp', 'tp'))
All inputs are finite; a program needn't handle non-finite values.
Results may differ from a plain program's by a relative error of at most 0.009.
The roundings to bfloat16 on the way count: a program that leaves them out, or rounds other values in their place, can miss the bound.
Values may be sent and summed in bfloat16 or wider, within the bound.
A program may use at most 64 MiB of HBM per device.

v0:
```python
import jax
import jax.numpy as jnp
from jax import lax
from jax.sharding import Mesh
from jax.sharding import PartitionSpec as P

HD = 64
GRID_W = 128
SP_TP = ("sp_0", "sp_1", "tp")
SP = ("sp_0", "sp_1")


EPS = 1e-06
THETA = 10000.0


def by_axis(shard, axes):
    for axis in axes:
        shard = lax.psum(shard, axis)
    return shard


def laid_out(blocks, dim):
    blocks = jnp.moveaxis(blocks, 0, dim)
    lengths = blocks.shape
    return blocks.reshape(*lengths[:dim], lengths[dim] * lengths[dim + 1], *lengths[dim + 2 :])


def copy_for_each(shard, axis):
    copies = jnp.broadcast_to(shard, (lax.axis_size(axis), *shard.shape))
    return lax.all_to_all(copies, axis, split_axis=0, concat_axis=0, tiled=True)


def gather_directly(shard, axis, dim):
    return laid_out(copy_for_each(shard, axis), dim)


def side_by_side(arrays, axis, dim, along):
    ends, at = ([], 0)
    for a in arrays[:-1]:
        at += a.shape[along]
        ends.append(at)
    both = jnp.concatenate(arrays, axis=along)
    return tuple(jnp.split(lax.all_gather(both, axis, axis=dim, tiled=True), ends, axis=along))


def modulate(row_block, gain_vec, shift_rows, scale_rows):
    values = row_block.astype(jnp.float32)
    normed = (
        values
        * lax.rsqrt(jnp.mean(values * values, axis=-1, keepdims=True) + EPS)
        * gain_vec.astype(jnp.float32)
    )
    return (normed * (1.0 + scale_rows) + shift_rows).astype(jnp.bfloat16)


def head_norm(raw_proj, gain_vec):
    samples, tokens, width = raw_proj.shape
    pieces = raw_proj.reshape(samples, tokens, width // HD, HD)
    normed = (
        pieces
        * lax.rsqrt(jnp.mean(pieces * pieces, axis=-1, keepdims=True) + EPS)
        * gain_vec.astype(jnp.float32)
    )
    return normed.transpose(0, 2, 1, 3)


def rotate(vector, positions):
    pairs_count = vector.shape[-1] // 4
    grid_row = (positions // GRID_W).astype(jnp.float32)
    grid_col = (positions % GRID_W).astype(jnp.float32)
    inverse = THETA ** (-jnp.arange(pairs_count, dtype=jnp.float32) / pairs_count)
    angles = jnp.concatenate([grid_row[:, None] * inverse, grid_col[:, None] * inverse], axis=-1)
    cosine = jnp.cos(angles)
    sine_val = jnp.sin(angles)
    first_half = vector[..., 0::2]
    second_half = vector[..., 1::2]
    turned = jnp.stack(
        [
            first_half * cosine - second_half * sine_val,
            first_half * sine_val + second_half * cosine,
        ],
        axis=-1,
    )
    return turned.reshape(vector.shape)


def split_heads(rows):
    samples, tokens, width = rows.shape
    return rows.reshape(samples, tokens, width // HD, HD).transpose(0, 2, 1, 3)


def on_device(
    latent,
    cond,
    cond_ctx,
    context,
    norm_gain,
    mod_shift,
    mod_scale,
    mod_gate,
    w_query,
    w_key,
    w_value,
    q_gain,
    k_gain,
    ctx_lift,
    w_out,
):
    samples = latent.shape[0]
    active = jax.nn.silu(
        jnp.concatenate([cond, cond_ctx[None, :]], axis=0).astype(jnp.float32)
    ).astype(jnp.bfloat16)
    partial_mods = tuple(
        (
            jnp.dot(active, weight, preferred_element_type=jnp.float32)
            for weight in (mod_shift, mod_scale, mod_gate)
        )
    )
    col_width = mod_shift.shape[1]
    offset = lax.axis_index("tp") * col_width
    blank = jnp.zeros((active.shape[0], col_width * lax.axis_size("tp")), jnp.float32)
    placed = tuple(
        (lax.dynamic_update_slice(blank, term, (jnp.int32(0), offset)) for term in partial_mods)
    )
    shift_rows, scale_rows, gate_rows = jax.tree.map(lambda part: by_axis(part, SP_TP), placed)
    modulated = modulate(
        latent, norm_gain, shift_rows[:samples, None, :], scale_rows[:samples, None, :]
    )
    ctx_mod = modulate(context, norm_gain, shift_rows[samples], scale_rows[samples])
    q_width = w_query.shape[1]
    k_width = w_key.shape[1]
    w_joint = jnp.concatenate([w_query, w_key, w_value], axis=1)
    projected = jnp.einsum(
        "srd,dc->src",
        gather_directly(modulated, "tp", 1),
        w_joint,
        preferred_element_type=jnp.float32,
    )
    tokens = projected.shape[1]
    k_heads = k_width // HD
    group_size = q_width // k_width
    positions = lax.axis_index(SP) * tokens + jnp.arange(tokens, dtype=jnp.int32)
    queries = rotate(head_norm(projected[..., :q_width], q_gain), positions).astype(jnp.bfloat16)
    queries = queries.reshape(samples, k_heads, group_size, tokens, HD)
    key_rows = rotate(
        head_norm(projected[..., q_width : q_width + k_width], k_gain), positions
    ).astype(jnp.bfloat16)
    value_rows = split_heads(projected[..., q_width + k_width :].astype(jnp.bfloat16))
    ctx_proj = jnp.einsum(
        "srd,dc->src", ctx_mod, w_joint[:, q_width:], preferred_element_type=jnp.float32
    )
    ctx_keys = head_norm(ctx_proj[..., :k_width], k_gain).astype(jnp.bfloat16)
    ctx_values = split_heads(ctx_proj[..., k_width:].astype(jnp.bfloat16))
    lift_table = ctx_lift.reshape(1, k_heads, group_size, 1, 1)
    factor = HD ** (-0.5)

    def absorb(state_now, key_block, value_block, score_lift):
        best_old, weight_sum, accumulated = state_now
        scores = (
            jnp.einsum("skgtd,skrd->skgtr", queries, key_block, preferred_element_type=jnp.float32)
            * factor
            + score_lift
        )
        peak = jnp.maximum(best_old, jnp.max(scores, axis=-1))
        weights = jnp.exp(scores - peak[..., None])
        rescale = jnp.exp(best_old - peak)
        weight_sum = weight_sum * rescale + jnp.sum(weights, axis=-1)
        accumulated = accumulated * rescale[..., None] + jnp.einsum(
            "skgtr,skrd->skgtd",
            weights.astype(jnp.bfloat16),
            value_block,
            preferred_element_type=jnp.float32,
        )
        return (peak, weight_sum, accumulated)

    stat_shape = (samples, k_heads, group_size, tokens)
    state_now = (
        jnp.full(stat_shape, -1e30, jnp.float32),
        jnp.zeros(stat_shape, jnp.float32),
        jnp.zeros(stat_shape + (HD,), jnp.float32),
    )
    all_ctx_keys, all_ctx_values = side_by_side((ctx_keys, ctx_values), SP, 2, 0)
    state_now = absorb(state_now, all_ctx_keys, all_ctx_values, lift_table)
    key_piece, value_piece = side_by_side((key_rows, value_rows), SP, 2, 0)
    block_count = key_piece.shape[2] // tokens
    key_blocks = jnp.moveaxis(key_piece.reshape(samples, k_heads, block_count, tokens, HD), 2, 0)
    value_blocks = jnp.moveaxis(
        value_piece.reshape(samples, k_heads, block_count, tokens, HD), 2, 0
    )

    def step_block(carry, blocks):
        return (absorb(carry, blocks[0], blocks[1], 0.0), None)

    state_out, unused = lax.scan(step_block, state_now, (key_blocks, value_blocks))
    state_now = state_out
    best_old, weight_sum, accumulated = state_now
    attended = (accumulated / weight_sum[..., None]).astype(jnp.bfloat16)
    head_rows = attended.transpose(0, 3, 1, 2, 4).reshape(samples, tokens, q_width)
    projected_out = jnp.einsum(
        "srq,qd->srd",
        lax.all_to_all(head_rows, "tp", split_axis=1, concat_axis=2, tiled=True),
        w_out,
        preferred_element_type=jnp.float32,
    )
    return (latent.astype(jnp.float32) + gate_rows[:samples, None, :] * projected_out).astype(
        jnp.bfloat16
    )


def solution(mesh):
    torus = Mesh(
        mesh.devices.reshape(4, 4, mesh.shape["tp"], mesh.shape["dp"]), ("sp_0", "sp_1", "tp", "dp")
    )
    in_specs = (
        P("dp", SP_TP, None),
        P("dp", SP),
        P(SP),
        P("dp", SP, None),
        P(),
        P(SP, "tp"),
        P(SP, "tp"),
        P(SP, "tp"),
        P(None, "tp"),
        P(None, "tp"),
        P(None, "tp"),
        P(),
        P(),
        P("tp"),
        P(),
    )
    out_specs = P("dp", SP_TP, None)
    return jax.shard_map(
        on_device, mesh=torus, in_specs=in_specs, out_specs=out_specs, check_vma=False
    )
```

profile of v0, /device:TPU:0, one launch (start us, length us, event | category | flops | bytes accessed | tf_op | source)
XLA Modules:
  0.0 279.6 jit_solution(13613016184180509849)
XLA Ops:
  11.7 18.8 %all-reduce.2 = (f32[2,2048]{1,0:T(2,128)S(1)}, f32[2,2048]{1,0:T(2,128)S(1)}, f32[2,2048]{1,0:T(2,128)S(1)}) all-reduce(f32[2,2048]{1,0:T(2,128)S(1)} %convolution_dynamic-update-slice_fusion, f32[2,2048]{1,0:T(2,128)S(1)} %convolution_dynamic-update-slice_fusion.1, ...), channel_id=1, replica_groups=mesh['sp_0'=4,'sp_1'=4,'tp'=4,'dp'=2] {'sp_0'}, use_global_device_ids=true, to_apply=%region_7.8 | all-reduce | flops 12288 | bytes 98304 | tf_op jit(solution)/shard_map/psum | solution.py:19
  30.5 17.8 %all-reduce.1 = (f32[2,2048]{1,0:T(2,128)S(1)}, f32[2,2048]{1,0:T(2,128)S(1)}, f32[2,2048]{1,0:T(2,128)S(1)}) all-reduce(f32[2,2048]{1,0:T(2,128)S(1)} %get-tuple-element.93, f32[2,2048]{1,0:T(2,128)S(1)} %get-tuple-element.94, f32[2,2048]{1,0:T(2,128)S(1)} %get-tuple-element.95), channel_id=1, replica_groups=mesh['sp_0'=4,'sp_1'=4,'tp'=4,'dp'=2] {'sp_1'}, use_global_device_ids=true, to_apply=%region_8.9 | all-reduce | flops 12288 | bytes 98304 | tf_op jit(solution)/shard_map/psum | solution.py:19
  48.2 18.0 %all-reduce = (f32[2,2048]{1,0:T(2,128)S(1)}, f32[2,2048]{1,0:T(2,128)S(1)}, f32[2,2048]{1,0:T(2,128)}) all-reduce(f32[2,2048]{1,0:T(2,128)S(1)} %get-tuple-element.90, f32[2,2048]{1,0:T(2,128)S(1)} %get-tuple-element.91, f32[2,2048]{1,0:T(2,128)S(1)} %get-tuple-element.92), channel_id=1, replica_groups=mesh['sp_0'=4,'sp_1'=4,'tp'=4,'dp'=2] {'tp'}, use_global_device_ids=true, to_apply=%region_9.10 | all-reduce | flops 12288 | bytes 98304 | tf_op jit(solution)/shard_map/psum | solution.py:19
  70.4 3.8 %all-to-all-start = ((bf16[4,1,192,2048]{3,2,1,0:T(8,128)(2,1)}), bf16[4,1,192,2048]{3,2,1,0:T(8,128)(2,1)S(1)}, u32[]{:S(2)}, u32[]{:S(2)}) async-start(bf16[4,1,192,2048]{3,2,1,0:T(8,128)(2,1)} %broadcast_in_dim.16), calls=%async_computation | async-start | bytes 6291456 | tf_op jit(solution)/shard_map/all_to_all | solution.py:31
  79.3 21.8 %all-to-all-done = bf16[4,1,192,2048]{3,2,1,0:T(8,128)(2,1)S(1)} async-done(((bf16[4,1,192,2048]{3,2,1,0:T(8,128)(2,1)}), bf16[4,1,192,2048]{3,2,1,0:T(8,128)(2,1)S(1)}, u32[]{:S(2)}, u32[]{:S(2)}) %all-to-all-start) | async-done | bytes 3145760 | tf_op jit(solution)/shard_map/all_to_all | solution.py:31
  102.8 4.1 %fusion.40 = f32[1,768,384]{1,2,0:T(8,128)S(1)} fusion(bf16[768,2048]{1,0:T(8,128)(2,1)} %bitcast.171, bf16[2048,64]{1,0:T(8,128)(2,1)} %copy.55, bf16[2048,64]{1,0:T(8,128)(2,1)} %copy.54, bf16[2048,256]{1,0:T(8,128)(2,1)} %param.25), kind=kOutput, calls=%fused_computation.46 | convolution fusion | flops 1212678144 | bytes 5898240 | tf_op jit(solution)/shard_map/srd,dc->src/dot_general | solution.py:134
  109.2 21.5 %all_gather.6 = bf16[2,1,512,64]{3,2,1,0:T(8,128)(2,1)S(1)} all-gather(bf16[2,1,32,64]{3,2,1,0:T(8,128)(2,1)S(1)} %pad_maximum_fusion.4), channel_id=1, replica_groups=mesh['sp_0'=4,'sp_1'=4,'tp'=4,'dp'=2] {'sp_0','sp_1'}, dimensions={2}, use_global_device_ids=true | all-gather | bytes 139264 | tf_op jit(solution)/shard_map/all_gather | solution.py:44
  136.5 17.2 %all-gather.2.cloned.1.call-done = bf16[2,1,12288,64]{2,3,1,0:T(8,128)(2,1)} async-done(((bf16[2,1,768,64]{2,3,1,0:T(8,128)(2,1)}), bf16[2,1,12288,64]{2,3,1,0:T(8,128)(2,1)}) %all-gather.2.cloned.1.call-update) | async-done | bytes 3145744 | tf_op jit(solution)/shard_map/all_gather | solution.py:44
  157.3 93.4 %while.14 = (s32[]{:T(128)}, f32[1,1,4,768]{3,2,1,0:T(4,128)S(1)}, f32[1,1,4,768]{3,2,1,0:T(4,128)S(1)}, f32[1,1,4,768,64]{3,4,2,1,0:T(8,128)S(1)}, bf16[16,1,1,...) while((s32[]{:T(128)}, f32[1,1,4,768]{3,2,1,0:T(4,128)S(1)}, ...), condition=%wide.region_19.20_spmd, body=%wide.region_16.19_spmd.sunk | while | flops 623256576 | bytes 30671448 | solution.py:195
  163.1 2.3 bitcast_reduce_fusion.2
  169.0 2.3 bitcast_reduce_fusion.2
  174.8 2.3 bitcast_reduce_fusion.2
  186.5 2.3 bitcast_reduce_fusion.2
  198.1 2.3 bitcast_reduce_fusion.2
  209.8 2.3 bitcast_reduce_fusion.2
  221.5 2.3 bitcast_reduce_fusion.2
  227.3 2.3 bitcast_reduce_fusion.2
  233.2 2.3 bitcast_reduce_fusion.2
  239.0 2.3 bitcast_reduce_fusion.2
  244.8 2.3 bitcast_reduce_fusion.2
  252.1 3.1 %reduce.15 = bf16[768,256]{1,0:T(8,128)(2,1)S(1)} reduce(bf16[768,1,256]{2,1,0:T(2,128)(2,1)S(1)} %bitcast.172, bf16[]{:T(256)} %broadcast.434), dimensions={1}, to_apply=%bitcast.129.reduce_sub_computation | reduce | bytes 786434
  256.1 4.2 %all-to-all-start.1 = ((bf16[4,2,24576]{2,1,0:T(2,128)(2,1)}), bf16[4,2,24576]{2,1,0:T(2,128)(2,1)S(1)}, u32[]{:S(2)}, u32[]{:S(2)}) async-start(bf16[4,2,24576]{2,1,0:T(2,128)(2,1)} %reshape.681), calls=%async_computation.1 | async-start | bytes 786432 | tf_op jit(solution)/shard_map/all_to_all | solution.py:202
  260.3 7.5 %all-to-all-done.1 = bf16[4,2,24576]{2,1,0:T(2,128)(2,1)S(1)} async-done(((bf16[4,2,24576]{2,1,0:T(2,128)(2,1)}), bf16[4,2,24576]{2,1,0:T(2,128)(2,1)S(1)}, u32[]{:S(2)}, u32[]{:S(2)}) %all-to-all-start.1) | async-done | bytes 393248 | tf_op jit(solution)/shard_map/all_to_all | solution.py:202
  268.7 4.1 %fusion.28 = bf16[1,192,2048]{2,1,0:T(8,128)(2,1)} fusion(bf16[192,1024]{1,0:T(8,128)(2,1)S(1)} %bitcast.181, bf16[1024,2048]{1,0:T(8,128)(2,1)} %param.31, bf16[1,192,2048]{2,1,0:T(8,128)(2,1)S(1)} %copy-done.2, f32[2048]{0:T(1024)S(1)} %bitcast.184), kind=kOutput, calls=%fused_computation.30 | convolution fusion | flops 806879232 | bytes 6168576 | tf_op jit(solution)/shard_map/srq,qd->srd/dot_general | solution.py:200
  (184 shorter events, 97.7 us)
Async XLA Ops:
  6.5 2.1 copy-start
  70.4 5.8 %copy-start.3 = (bf16[2048,64]{0,1:T(8,128)(2,1)S(1)}, bf16[2048,64]{0,1:T(8,128)(2,1)}, u32[]{:S(2)}) copy-start(bf16[2048,64]{0,1:T(8,128)(2,1)} %param.27) | copy-start | bytes 786436
  70.4 30.7 %all-to-all-start = ((bf16[4,1,192,2048]{3,2,1,0:T(8,128)(2,1)}), bf16[4,1,192,2048]{3,2,1,0:T(8,128)(2,1)S(1)}, u32[]{:S(2)}, u32[]{:S(2)}) async-start(bf16[4,1,192,2048]{3,2,1,0:T(8,128)(2,1)} %broadcast_in_dim.16), calls=%async_computation | async-start | bytes 6291456 | tf_op jit(solution)/shard_map/all_to_all | solution.py:31
  74.2 79.4 %all-gather.2.cloned.1.call-start = ((), (), s32[]{:S(2)}) async-start(), calls=%async_computation.2 | async-start | bytes 3342336 | tf_op jit(solution)/shard_map/all_gather | solution.py:44
  101.0 1.7 copy-start.1
  102.7 4.2 %copy-start.13 = (f32[64]{0:T(128)S(1)}, f32[64]{0:T(128)}, u32[]{:S(2)}) copy-start(f32[64]{0:T(128)} %convert_element_type.131) | copy-start | bytes 772
  102.7 4.4 %copy-start.7 = (f32[1,1,768,16]{2,3,1,0:T(8,128)S(1)}, f32[1,1,768,16]{2,3,1,0:T(8,128)}, u32[]{:S(2)}) copy-start(f32[1,1,768,16]{2,3,1,0:T(8,128)} %get-tuple-element.115) | copy-start | bytes 147460
  102.7 4.4 %copy-start.8 = (f32[1,1,768,16]{2,3,1,0:T(8,128)S(1)}, f32[1,1,768,16]{2,3,1,0:T(8,128)}, u32[]{:S(2)}) copy-start(f32[1,1,768,16]{2,3,1,0:T(8,128)} %get-tuple-element.120) | copy-start | bytes 147460
  102.7 5.7 %copy-start.14 = (bf16[64]{0:T(256)(128)(2,1)S(1)}, bf16[64]{0:T(256)(128)(2,1)}, u32[]{:S(2)}) copy-start(bf16[64]{0:T(256)(128)(2,1)} %param.28) | copy-start | bytes 388
  102.7 5.7 %copy-start.9 = (bf16[1,32,2048]{2,1,0:T(8,128)(2,1)S(1)}, bf16[1,32,2048]{2,1,0:T(8,128)(2,1)}, u32[]{:S(2)}) copy-start(bf16[1,32,2048]{2,1,0:T(8,128)(2,1)} %param.20) | copy-start | bytes 393220
  102.7 5.8 %copy-start.4 = (bf16[2048,64]{0,1:T(8,128)(2,1)S(1)}, bf16[2048,64]{0,1:T(8,128)(2,1)}, u32[]{:S(2)}) copy-start(bf16[2048,64]{0,1:T(8,128)(2,1)} %param.26) | copy-start | bytes 786436
  102.7 5.8 %copy-start.10 = (f32[1,2048]{1,0:T(1,128)S(1)}, f32[1,2048]{1,0:T(1,128)}, u32[]{:S(2)}) copy-start(f32[1,2048]{1,0:T(1,128)} %get-tuple-element.124) | copy-start | bytes 24580
  106.8 23.9 %copy-start.5 = (f32[768,16]{0,1:T(8,128)S(1)}, f32[768,16]{0,1:T(8,128)}, u32[]{:S(2)}) copy-start(f32[768,16]{0,1:T(8,128)} %get-tuple-element.116) | copy-start | bytes 147460
  106.8 23.9 %copy-start.6 = (f32[768,16]{0,1:T(8,128)S(1)}, f32[768,16]{0,1:T(8,128)}, u32[]{:S(2)}) copy-start(f32[768,16]{0,1:T(8,128)} %get-tuple-element.119) | copy-start | bytes 147460
  131.4 1.3 copy-start.12
  250.7 9.6 %copy-start.11 = (f32[2,2048]{1,0:T(2,128)S(1)}, f32[2,2048]{1,0:T(2,128)}, u32[]{:S(2)}) copy-start(f32[2,2048]{1,0:T(2,128)} %get-tuple-element.89) | copy-start | bytes 49156
  252.1 16.6 %copy-start.2 = (bf16[1,192,2048]{2,1,0:T(8,128)(2,1)S(1)}, bf16[1,192,2048]{2,1,0:T(8,128)(2,1)}, u32[]{:S(2)}) copy-start(bf16[1,192,2048]{2,1,0:T(8,128)(2,1)} %param.17) | copy-start | bytes 2359300
  256.1 11.8 %all-to-all-start.1 = ((bf16[4,2,24576]{2,1,0:T(2,128)(2,1)}), bf16[4,2,24576]{2,1,0:T(2,128)(2,1)S(1)}, u32[]{:S(2)}, u32[]{:S(2)}) async-start(bf16[4,2,24576]{2,1,0:T(2,128)(2,1)} %reshape.681), calls=%async_computation.1 | async-start | bytes 786432 | tf_op jit(solution)/shard_map/all_to_all | solution.py:202
Sparse Core Ops, SparseCore 0:
  108.5 45.0 all-gather.1
where the time goes:
time: 281 us; the launch traced here: 280 us
  matrix products  81.1 us (29%)
  blocking collectives  76 us (27%)
  waiting for transfers between devices  46.5 us (17%)
  other arithmetic  38.4 us (14%)
  local copies, waits for them, and re-layouts  14.9 us (5%)
  between operations  13.9 us (5%)
  starting transfers between devices  8.12 us (3%)
    psum x3, blocking collectives, by_axis(): shard = lax.psum(shard, axis)  54.5 us
    dot_general x17, matrix products, absorb(): jnp.einsum('skgtd,skrd->skgtr', queries, key_block, preferred_element_typ...  38.1 us
    dot_general x17, matrix products, absorb(): jnp.einsum('skgtr,skrd->skgtd', weights.astype(jnp.bfloat16), value_block...  31.5 us
    reduce_sum x17, other arithmetic, absorb(): weight_sum = weight_sum * rescale + jnp.sum(weights, axis=-1)  26.1 us
    all_to_all x1, waiting for transfers between devices, copy_for_each(): return lax.all_to_all(copies, axis, split_axis=0, concat_axis=0, tiled=True)  21.8 us
    all_gather x1, blocking collectives, side_by_side(): lax.all_gather(both, axis, axis=dim, tiled=True)  21.5 us
    all_gather x1, waiting for transfers between devices, side_by_side(): lax.all_gather(both, axis, axis=dim, tiled=True)  17.2 us
    all_to_all x1, waiting for transfers between devices, on_device(): lax.all_to_all(head_rows, 'tp', split_axis=1, concat_axis=2, tiled=True)  7.5 us
  transfers between devices with their start and end apart: 3, of which 3 were waited for; matrix products, arithmetic and copies ran while one was open for 4% of the time, Pallas kernels for 0%

commit v1 on v0

v1 whole, which is shorter than its diff:
```python
import functools

import jax
import jax.numpy as jnp
import numpy as np
from jax import lax
from jax.experimental import pallas as pl
from jax.experimental.pallas import tpu as pltpu
from jax.sharding import PartitionSpec as P

MESH = pl.DeviceIdType.MESH
HD = 64
GRID_W = 128
EPS = 1e-06
THETA = 10000.0
LOG2E = 1.4426950408889634
N_SP = 16
N_TP = 4
F32 = jnp.float32
BF16 = jnp.bfloat16
VMEM = pl.BlockSpec(memory_space=pltpu.VMEM)
ANY = pl.BlockSpec(memory_space=pl.ANY)
SMEM = pl.BlockSpec(memory_space=pltpu.SMEM)
LIMIT = 60 * 2**20


def angle_table():
    i = (np.arange(HD) // 2) % 16
    f = (THETA ** (-(i.astype(np.float32)) / np.float32(16))).astype(np.float32)
    table = np.repeat(f[:, None], GRID_W, axis=1)
    table[32:] = table[32:] * np.arange(GRID_W, dtype=np.float32)[None, :]
    return table.astype(np.float32)


def tall(x):
    return jnp.concatenate([x, jnp.zeros_like(x)], axis=0)


def project_kernel(
    lat, cond, condc, ctx, gain, m_shift, m_scale, m_gate, wq, wk, wv, qg, kg, table,
    q_out, kv_out, ctx_out, gate_out,
    xbuf, part, psum_in, mine, full, wall, ubuf, raw, cosb, sinb, scl, sft, cown, cbuf,
    x_send, x_recv, p_send, p_recv, t_send, t_recv, c_send, c_recv,
):
    sp = lax.axis_index("sp")
    tp = lax.axis_index("tp")
    rows = lat.shape[0]
    half = rows // 2

    def sp_at(k):
        return {"sp": lax.rem(sp + k, N_SP)}

    def tp_at(k):
        return {"tp": lax.rem(tp + k, N_TP)}

    barrier = pltpu.get_barrier_semaphore()
    for k in range(1, N_SP):
        pl.semaphore_signal(barrier, inc=1, device_id=sp_at(k), device_id_type=MESH)
    for k in range(1, N_TP):
        pl.semaphore_signal(barrier, inc=1, device_id=tp_at(k), device_id_type=MESH)
    pl.semaphore_wait(barrier, N_SP - 1 + N_TP - 1)

    def send(src, dst, s_sem, r_sem, target):
        return pltpu.make_async_remote_copy(
            src_ref=src, dst_ref=dst, send_sem=s_sem, recv_sem=r_sem,
            device_id=target, device_id_type=MESH,
        )

    h0, h1 = pl.ds(0, half), pl.ds(half, half)
    r0 = send(lat.at[h0], xbuf.at[0, h0], x_send.at[0], x_recv.at[0], tp_at(1))
    l1 = send(lat.at[h1], xbuf.at[2, h1], x_send.at[1], x_recv.at[1], tp_at(3))
    r1 = send(lat.at[h1], xbuf.at[0, h1], x_send.at[2], x_recv.at[2], tp_at(1))
    l0 = send(lat.at[h0], xbuf.at[2, h0], x_send.at[3], x_recv.at[3], tp_at(3))
    f0 = send(xbuf.at[0, h0], xbuf.at[1, h0], x_send.at[4], x_recv.at[4], tp_at(1))
    f1 = send(xbuf.at[2, h1], xbuf.at[1, h1], x_send.at[5], x_recv.at[5], tp_at(3))
    r0.start()
    l1.start()

    at = lax.broadcasted_iota(jnp.int32, (16, 128), 0)
    given = jnp.where(
        at == 0,
        jnp.broadcast_to(cond[...].astype(F32), (16, 128)),
        jnp.where(at == 1, jnp.broadcast_to(condc[...].astype(F32), (16, 128)), 0.0),
    )
    active = (given / (1.0 + jnp.exp(-given))).astype(BF16)
    for k, weight in enumerate((m_shift, m_scale, m_gate)):
        product = jnp.dot(active, weight[...], preferred_element_type=F32)
        for r in range(2):
            for c in range(4):
                i = r * 12 + k * 4 + c
                part[i : i + 1, :] = product[r : r + 1, c * 128 : (c + 1) * 128]
    p_copies = [
        send(part, psum_in.at[k - 1], p_send.at[k - 1], p_recv.at[k - 1], sp_at(k))
        for k in range(1, N_SP)
    ]
    for copy in p_copies:
        copy.start()

    wall[:, 0:256] = wq[...]
    wall[:, 256:384] = jnp.concatenate([wk[...], wv[...]], axis=1)
    row_id = lax.broadcasted_iota(jnp.int32, (HD, GRID_W), 0)
    even = lax.rem(row_id, 2) == 0
    for g in range(6):
        grid_row = (sp * 6 + g).astype(F32)
        angle = table[...] * jnp.where(row_id < 32, grid_row, 1.0)
        cosb[g] = jnp.cos(angle)
        sine = jnp.sin(angle)
        sinb[g] = jnp.where(even, -sine, sine)

    for copy in p_copies:
        copy.wait_recv()
    total = part[...]
    for k in range(N_SP - 1):
        total = total + psum_in[k]
    mine[...] = total
    t_copies = [
        send(mine, full.at[tp], t_send.at[k - 1], t_recv.at[k - 1], tp_at(k))
        for k in range(1, N_TP)
    ]
    for copy in t_copies:
        copy.start()
    r1.start()
    l0.start()
    full[tp] = total
    for copy in t_copies:
        copy.wait_recv()

    def vector(r, k):
        pieces = [
            full[t, r * 12 + k * 4 + c : r * 12 + k * 4 + c + 1, :]
            for t in range(N_TP)
            for c in range(4)
        ]
        return jnp.concatenate(pieces, axis=1)

    width = lat.shape[1]
    for r in range(2):
        scaled = gain[...].astype(F32) * (1.0 + vector(r, 1))
        scl[r] = jnp.broadcast_to(scaled, (8, width))
        sft[r] = jnp.broadcast_to(vector(r, 0), (8, width))
    gate_out[...] = vector(0, 2)

    def modulate(src, r, count):
        values = src.astype(F32)
        inverse = lax.rsqrt(jnp.mean(values * values, axis=-1, keepdims=True) + EPS)
        normed = (values * inverse).reshape(count // 8, 8, width)
        return (normed * scl[r][None] + sft[r][None]).reshape(count, width).astype(BF16)

    uc = modulate(ctx[...], 1, ctx.shape[0])
    craw = jnp.dot(uc, wall[:, 256:384], preferred_element_type=F32)
    lane = lax.broadcasted_iota(jnp.int32, craw.shape, 1)
    square = jnp.where(lane < HD, craw * craw, 0.0)
    mean = jnp.sum(square, axis=-1, keepdims=True) * (1.0 / HD)
    keys = craw * lax.rsqrt(mean + EPS) * jnp.concatenate(
        [kg[...].astype(F32).T, jnp.ones((1, HD), F32)], axis=1
    )
    cown[...] = jnp.where(lane < HD, keys, craw).astype(BF16)
    c_copies = [
        send(cown, cbuf.at[k - 1], c_send.at[k - 1], c_recv.at[k - 1], sp_at(k))
        for k in range(1, N_SP)
    ]
    for copy in c_copies:
        copy.start()

    def project(x, owner):
        @pl.loop(0, rows // 32)
        def _(i):
            at_rows = pl.ds(pl.multiple_of(i * 32, 32), 32)
            ubuf[at_rows, :] = modulate(x[at_rows, :], 0, 32)

        raw[pl.ds(pl.multiple_of(owner * rows, rows), rows), :] = jnp.dot(
            ubuf[...], wall[...], preferred_element_type=F32
        )

    project(lat, tp)
    r0.wait_recv()
    f0.start()
    l1.wait_recv()
    f1.start()
    r1.wait_recv()
    project(xbuf.at[0], lax.rem(tp + 3, N_TP))
    l0.wait_recv()
    project(xbuf.at[2], lax.rem(tp + 1, N_TP))
    f0.wait_recv()
    f1.wait_recv()
    project(xbuf.at[1], lax.rem(tp + 2, N_TP))

    def turned(x, gain_column, g):
        square = jnp.sum(x * x, axis=0, keepdims=True) * (1.0 / HD)
        normed = x * lax.rsqrt(square + EPS) * gain_column
        up = pltpu.roll(normed, HD - 1, axis=0)
        down = pltpu.roll(normed, 1, axis=0)
        return normed * cosb[g] + jnp.where(even, up, down) * sinb[g]

    q_gain = qg[...].astype(F32)
    k_gain = kg[...].astype(F32)
    scale = LOG2E * HD ** (-0.5)
    for g in range(6):
        block = raw[g * 128 : (g + 1) * 128, :]
        for pair in range(2):
            side = block[:, pair * 128 : (pair + 1) * 128].T
            for h in range(2):
                q = turned(side[h * HD : (h + 1) * HD], q_gain, g)
                lanes = g * 512 + (pair * 2 + h) * 128
                q_out[:, lanes : lanes + 128] = (q * scale).astype(BF16)
        side = block[:, 256:384].T
        k = turned(side[0:HD], k_gain, g).T
        kv_out[g * 64 : (g + 1) * 64, :] = jnp.concatenate([k[0:64], k[64:128]], axis=1).astype(
            BF16
        )
    for s in range(2):
        order = [(g, p) for p in range(2) for g in (3 * s, 3 * s + 1, 3 * s + 2)]
        for b in range(3):
            pieces = [
                raw[g * 128 + p * 64 : g * 128 + p * 64 + 64, 256:384]
                for g, p in order[2 * b : 2 * b + 2]
            ]
            side = jnp.concatenate(pieces, axis=0).T
            at_row = 384 + (3 * s + b) * 64
            kv_out[at_row : at_row + 64, :] = side[HD : 2 * HD].astype(BF16)

    for copy in c_copies:
        copy.wait_recv()
    ctx_out[0:32, :] = cown[...]
    for k in range(N_SP - 1):
        ctx_out[32 * (k + 1) : 32 * (k + 2), :] = cbuf[k]
    for copy in p_copies + t_copies + c_copies + [r0, l1, r1, l0, f0, f1]:
        copy.wait_send()


def run_project(lat, cond, condc, ctx, gain, ms, mc, mg, wq, wk, wv, qg, kg):
    rows, width = lat.shape
    dma = pltpu.SemaphoreType.DMA
    return pl.pallas_call(
        project_kernel,
        name="project",
        out_shape=(
            jax.ShapeDtypeStruct((HD, 3072), BF16),
            jax.ShapeDtypeStruct((768, 128), BF16),
            jax.ShapeDtypeStruct((512, 128), BF16),
            jax.ShapeDtypeStruct((1, width), F32),
        ),
        in_specs=[VMEM] * 14,
        out_specs=(VMEM,) * 4,
        scratch_shapes=[
            pltpu.VMEM((3, rows, width), BF16),
            pltpu.VMEM((24, 128), F32),
            pltpu.VMEM((N_SP - 1, 24, 128), F32),
            pltpu.VMEM((24, 128), F32),
            pltpu.VMEM((N_TP, 24, 128), F32),
            pltpu.VMEM((width, 384), BF16),
            pltpu.VMEM((rows, width), BF16),
            pltpu.VMEM((768, 384), F32),
            pltpu.VMEM((6, HD, GRID_W), F32),
            pltpu.VMEM((6, HD, GRID_W), F32),
            pltpu.VMEM((2, 8, width), F32),
            pltpu.VMEM((2, 8, width), F32),
            pltpu.VMEM((32, 128), BF16),
            pltpu.VMEM((N_SP - 1, 32, 128), BF16),
            dma((6,)), dma((6,)), dma((15,)), dma((15,)),
            dma((3,)), dma((3,)), dma((15,)), dma((15,)),
        ],
        compiler_params=pltpu.CompilerParams(
            collective_id=0, has_side_effects=True, vmem_limit_bytes=LIMIT
        ),
    )(lat, cond, condc, ctx, gain, ms, mc, mg, wq, wk, wv, qg, kg, jnp.asarray(angle_table()))


SLOTS = [
    (0, 0), (-1, 0), (1, 0), (0, -1), (0, 1), (2, 0), (-1, -1), (-1, 1),
    (1, -1), (1, 1), (0, 2), (2, -1), (2, 1), (-1, 2), (1, 2), (2, 2),
]
SENDS = [
    (0, 1, 1, 0), (0, 2, -1, 0), (0, 3, 0, 1), (0, 4, 0, -1),
    (1, 5, 1, 0), (1, 6, 0, 1), (1, 7, 0, -1),
    (2, 8, 0, 1), (2, 9, 0, -1),
    (3, 10, 0, 1),
    (5, 11, 0, 1), (5, 12, 0, -1),
    (7, 13, 0, -1), (8, 14, 0, 1), (12, 15, 0, -1),
]
TILE = 1024
VROWS = 80


def attend_kernel(
    q_ref, kv_own, ctx, lift, o_out, l_out, kv_all,
    kvbuf, acc, peak, pbuf, send_sem, recv_sem, keep_sem,
):
    sp = lax.axis_index("sp")
    y, z = lax.rem(sp, 4), lax.div(sp, 4)
    tiles = q_ref.shape[1] // TILE

    def near(dy, dz):
        return {"sp": lax.rem(z + dz + 4, 4) * 4 + lax.rem(y + dy + 4, 4)}

    barrier = pltpu.get_barrier_semaphore()
    for dy, dz in ((1, 0), (-1, 0), (0, 1), (0, -1)):
        pl.semaphore_signal(barrier, inc=1, device_id=near(dy, dz), device_id_type=MESH)
    pl.semaphore_wait(barrier, 4)

    sends = []
    for i, (here, there, dy, dz) in enumerate(SENDS):
        sends.append(
            pltpu.make_async_remote_copy(
                src_ref=kv_own if here == 0 else kvbuf.at[here],
                dst_ref=kvbuf.at[there],
                send_sem=send_sem.at[i],
                recv_sem=recv_sem.at[there],
                device_id=near(dy, dz),
                device_id_type=MESH,
            )
        )

    def start_from(slot):
        for copy, (here, _, _, _) in zip(sends, SENDS):
            if here == slot:
                copy.start()

    def arrival(slot):
        return next(copy for copy, (_, there, _, _) in zip(sends, SENDS) if there == slot)

    def keep(slot):
        src = kv_own if slot == 0 else kvbuf.at[slot]
        return pltpu.make_async_copy(src, kv_all.at[slot], keep_sem.at[slot])

    start_from(0)
    keep(0).start()
    kvbuf[0] = kv_own[...]

    lifts = jnp.concatenate([jnp.full((1, 128), lift[h] * LOG2E, F32) for h in range(4)], axis=1)
    lifts = jnp.concatenate([lifts] * (TILE // 512), axis=1)
    ones = jnp.ones((VROWS - HD, 768), BF16)

    def lanes(t):
        if isinstance(t, int):
            return pl.ds(t * TILE, TILE)
        return pl.ds(pl.multiple_of(t * TILE, TILE), TILE)

    cv = ctx[...].astype(F32).T[HD : 2 * HD].astype(BF16)
    cv = jnp.concatenate([cv, ones[:, 0:512]], axis=0)

    for t in range(tiles):
        scores = jnp.dot(ctx[...], tall(q_ref[:, lanes(t)]), preferred_element_type=F32) + lifts
        top = jnp.max(scores, axis=0, keepdims=True)
        peak[:, lanes(t)] = top
        weights = jnp.exp2(scores - top).astype(BF16)
        acc[:, lanes(t)] = jnp.dot(cv, weights, preferred_element_type=F32)

    def score(b, t, slot):
        q = q_ref[:, lanes(t)]
        left = tall(q)
        right = jnp.concatenate([jnp.zeros_like(q), q], axis=0)
        top = peak[:, lanes(t)]
        for s in range(2):
            k = kvbuf[b, pl.ds(s * 192, 192), :]
            for p, query in enumerate((left, right)):
                x = jnp.dot(k, query, preferred_element_type=F32)
                pbuf[slot, pl.ds(s * 384 + p * 192, 192), :] = jnp.exp2(x - top).astype(BF16)

    def value(b, t, slot):
        v = [kvbuf[b, pl.ds(384 + g * 64, 64), :] for g in range(6)]
        v = jnp.concatenate([jnp.concatenate(v, axis=1), ones], axis=0)
        acc[:, lanes(t)] += jnp.dot(v, pbuf[slot], preferred_element_type=F32)

    score(0, 0, 0)

    def step(b, carry):
        for t in range(tiles - 1):
            value(b, t, t % 2)
            score(b, t + 1, (t + 1) % 2)
        for slot in range(1, N_SP):

            @pl.when(b == slot - 1)
            def _(slot=slot):
                arrival(slot).wait_recv()
                start_from(slot)
                keep(slot).start()

        last = tiles - 1
        value(b, last, last % 2)
        score(jnp.minimum(b + 1, N_SP - 1), 0, 0)
        return carry

    lax.fori_loop(0, N_SP, step, 0)

    l_out[...] = acc[HD : HD + 8, :]
    for g in range(6):
        at_lanes = pl.ds(g * 512, 512)
        mean = acc[0:HD, at_lanes] / acc[HD : HD + 1, at_lanes]
        stack = jnp.concatenate([mean[:, h * 128 : (h + 1) * 128] for h in range(4)], axis=0)
        o_out[g * 128 : (g + 1) * 128, :] = stack.T.astype(BF16)
    for copy in sends:
        copy.wait_send()
    for slot in range(N_SP):
        keep(slot).wait()


def run_attend(q, kv, ctx, lift):
    dma = pltpu.SemaphoreType.DMA
    return pl.pallas_call(
        attend_kernel,
        name="attend",
        out_shape=(
            jax.ShapeDtypeStruct((768, 256), BF16),
            jax.ShapeDtypeStruct((8, 3072), F32),
            jax.ShapeDtypeStruct((N_SP, 768, 128), BF16),
        ),
        in_specs=[VMEM, VMEM, VMEM, SMEM],
        out_specs=(VMEM, VMEM, ANY),
        scratch_shapes=[
            pltpu.VMEM((N_SP, 768, 128), BF16),
            pltpu.VMEM((VROWS, 3072), F32),
            pltpu.VMEM((1, 3072), F32),
            pltpu.VMEM((2, 768, TILE), BF16),
            dma((len(SENDS),)),
            dma((N_SP,)),
            dma((N_SP,)),
        ],
        compiler_params=pltpu.CompilerParams(
            collective_id=1, has_side_effects=True, vmem_limit_bytes=LIMIT
        ),
    )(q, kv, ctx, lift)


def repair_kernel(
    l_ref, o_in, q_hbm, kv_hbm, ctx_hbm, lift, o_out,
    q_ref, kvbuf, ctx, acc, peak, o_buf, sem,
):
    safe = jnp.all(l_ref[...] < 2.0**100)

    @pl.when(jnp.logical_not(safe))
    def _():
        for src, dst in ((q_hbm, q_ref), (kv_hbm, kvbuf), (ctx_hbm, ctx)):
            copy = pltpu.make_async_copy(src, dst, sem)
            copy.start()
            copy.wait()
        wide = 512
        ones = jnp.ones((VROWS - HD, 768), BF16)
        lifts = jnp.concatenate(
            [jnp.full((1, 128), lift[h] * LOG2E, F32) for h in range(4)], axis=1
        )
        cv = ctx[...].astype(F32).T[HD : 2 * HD].astype(BF16)
        cv = jnp.concatenate([cv, ones[:, 0:512]], axis=0)

        @pl.loop(0, q_ref.shape[1] // wide)
        def _(t):
            lanes = pl.ds(pl.multiple_of(t * wide, wide), wide)
            q = q_ref[:, lanes]
            left = tall(q)
            right = jnp.concatenate([jnp.zeros_like(q), q], axis=0)
            scores = jnp.dot(ctx[...], left, preferred_element_type=F32) + lifts
            top = jnp.max(scores, axis=0, keepdims=True)
            peak[...] = top
            weights = jnp.exp2(scores - top).astype(BF16)
            acc[...] = jnp.dot(cv, weights, preferred_element_type=F32)

            @pl.loop(0, N_SP)
            def _(b):
                parts = []
                for s in range(2):
                    k = kvbuf[b, pl.ds(s * 192, 192), :]
                    for query in (left, right):
                        parts.append(jnp.dot(k, query, preferred_element_type=F32))
                x = jnp.concatenate(parts, axis=0)
                old = peak[...]
                new = jnp.maximum(old, jnp.max(x, axis=0, keepdims=True))
                peak[...] = new
                v = [kvbuf[b, pl.ds(384 + g * 64, 64), :] for g in range(6)]
                v = jnp.concatenate([jnp.concatenate(v, axis=1), ones], axis=0)
                weights = jnp.exp2(x - new).astype(BF16)
                acc[...] = acc[...] * jnp.exp2(old - new) + jnp.dot(
                    v, weights, preferred_element_type=F32
                )

            mean = acc[0:HD, :] / acc[HD : HD + 1, :]
            stack = jnp.concatenate([mean[:, h * 128 : (h + 1) * 128] for h in range(4)], axis=0)
            o_buf[...] = stack.T.astype(BF16)
            rows = pl.ds(pl.multiple_of(t * 128, 128), 128)
            copy = pltpu.make_async_copy(o_buf, o_out.at[rows], sem)
            copy.start()
            copy.wait()


def run_repair(l, o, q, kv_all, ctx, lift):
    return pl.pallas_call(
        repair_kernel,
        name="repair",
        out_shape=jax.ShapeDtypeStruct(o.shape, o.dtype),
        in_specs=[VMEM, ANY, ANY, ANY, ANY, SMEM],
        out_specs=ANY,
        input_output_aliases={1: 0},
        scratch_shapes=[
            pltpu.VMEM((HD, 3072), BF16),
            pltpu.VMEM((N_SP, 768, 128), BF16),
            pltpu.VMEM((512, 128), BF16),
            pltpu.VMEM((VROWS, 512), F32),
            pltpu.VMEM((1, 512), F32),
            pltpu.VMEM((128, 256), BF16),
            pltpu.SemaphoreType.DMA(()),
        ],
        compiler_params=pltpu.CompilerParams(vmem_limit_bytes=LIMIT),
    )(l, o, q, kv_all, ctx, lift)


def output_kernel(
    o_ref, w_hbm, lat, gate, out,
    wbuf, obuf, send_sem, recv_sem, w_sem,
):
    tp = lax.axis_index("tp")
    rows = lat.shape[0]

    def tp_at(k):
        return lax.rem(tp + k, N_TP)

    load = pltpu.make_async_copy(w_hbm, wbuf, w_sem)
    load.start()
    barrier = pltpu.get_barrier_semaphore()
    for k in range(1, N_TP):
        pl.semaphore_signal(barrier, inc=1, device_id={"tp": tp_at(k)}, device_id_type=MESH)
    pl.semaphore_wait(barrier, N_TP - 1)
    copies = []
    for k in range(1, N_TP):
        theirs = pl.ds(pl.multiple_of(tp_at(k) * rows, rows), rows)
        copies.append(
            pltpu.make_async_remote_copy(
                src_ref=o_ref.at[theirs], dst_ref=obuf.at[tp],
                send_sem=send_sem.at[k - 1], recv_sem=recv_sem.at[k - 1],
                device_id={"tp": tp_at(k)}, device_id_type=MESH,
            )
        )
        copies[-1].start()
    obuf[tp] = o_ref[pl.ds(pl.multiple_of(tp * rows, rows), rows), :]
    load.wait()
    for copy in copies:
        copy.wait_recv()
    wide = 512
    for n in range(out.shape[1] // wide):
        cols = slice(n * wide, (n + 1) * wide)
        total = None
        for t in range(N_TP):
            term = jnp.dot(
                obuf[t], wbuf[t * 256 : (t + 1) * 256, cols], preferred_element_type=F32
            )
            total = term if total is None else total + term
        out[:, cols] = (lat[:, cols].astype(F32) + gate[:, cols] * total).astype(BF16)
    for copy in copies:
        copy.wait_send()


def run_output(o, w_out, lat, gate):
    rows, width = lat.shape
    dma = pltpu.SemaphoreType.DMA
    return pl.pallas_call(
        output_kernel,
        name="output",
        out_shape=jax.ShapeDtypeStruct((rows, width), BF16),
        in_specs=[VMEM, ANY, VMEM, VMEM],
        out_specs=VMEM,
        scratch_shapes=[
            pltpu.VMEM(w_out.shape, BF16),
            pltpu.VMEM((N_TP, rows, 256), BF16),
            dma((N_TP - 1,)),
            dma((N_TP - 1,)),
            dma(()),
        ],
        compiler_params=pltpu.CompilerParams(
            collective_id=2, has_side_effects=True, vmem_limit_bytes=LIMIT
        ),
    )(o, w_out, lat, gate)


def on_device(
    latent, cond, cond_ctx, context, norm_gain, mod_shift, mod_scale, mod_gate,
    w_query, w_key, w_value, q_gain, k_gain, ctx_lift, w_out,
):
    lat = latent[0]
    q, kv, ctx, gate = run_project(
        lat, cond, cond_ctx[None, :], context[0], norm_gain[None, :],
        mod_shift, mod_scale, mod_gate, w_query, w_key, w_value,
        q_gain[:, None], k_gain[:, None],
    )
    o, l, kv_all = run_attend(q, kv, ctx, ctx_lift)
    o = run_repair(l, o, q, kv_all, ctx, ctx_lift)
    return run_output(o, w_out, lat, gate)[None]


def solution(mesh):
    in_specs = (
        P("dp", ("sp", "tp"), None),
        P("dp", "sp"),
        P("sp"),
        P("dp", "sp", None),
        P(),
        P("sp", "tp"),
        P("sp", "tp"),
        P("sp", "tp"),
        P(None, "tp"),
        P(None, "tp"),
        P(None, "tp"),
        P(),
        P(),
        P("tp"),
        P(),
    )
    return jax.shard_map(
        on_device, mesh=mesh, in_specs=in_specs,
        out_specs=P("dp", ("sp", "tp"), None), check_vma=False,
    )
```

time: 281 us -> 109 us (0.39)
  Pallas kernels: 0 us -> 98.7 us
  matrix products: 81.1 us -> 0 us
  blocking collectives: 76 us -> 0 us
  waiting for transfers between devices: 46.5 us -> 0 us
  other arithmetic: 38.4 us -> 0 us
  between operations: 13.9 us -> 0.04 us
  starting transfers between devices: 8.12 us -> 0 us
  local copies, waits for them, and re-layouts: 14.9 us -> 9.97 us
    pallas_call x0 -> x4, Pallas kernels: none -> 98.7 us  [the longest x1 45.6 us: run_attend(): pl.pallas_call(attend_kernel, name='attend', out_shape=(jax.ShapeDtypeStr...]
    dot_general x40 -> x0, matrix products: 81.1 us -> none  [the longest x17 38.1 us: absorb(): jnp.einsum('skgtd,skrd->skgtr', queries, key_block, preferred_element_typ...]
    psum x3 -> x0, blocking collectives: 54.5 us -> none  [by_axis(): shard = lax.psum(shard, axis)]
    all_to_all x2 -> x0, waiting for transfers between devices: 29.3 us -> none  [the longest x1 21.8 us: copy_for_each(): return lax.all_to_all(copies, axis, split_axis=0, concat_axis=0, tiled=True)]
    reduce_sum x22 -> x0, other arithmetic: 27.9 us -> none  [the longest x17 26.1 us: absorb(): weight_sum = weight_sum * rescale + jnp.sum(weights, axis=-1)]
    all_gather x1 -> x0, blocking collectives: 21.5 us -> none  [side_by_side(): lax.all_gather(both, axis, axis=dim, tiled=True)]
    all_gather x1 -> x0, waiting for transfers between devices: 17.2 us -> none  [side_by_side(): lax.all_gather(both, axis, axis=dim, tiled=True)]
    all_to_all x2 -> x0, starting transfers between devices: 8.08 us -> none  [the longest x1 4.25 us: on_device(): lax.all_to_all(head_rows, 'tp', split_axis=1, concat_axis=2, tiled=True)]
  transfers between devices with their start and end apart: 3 -> 0, of which waited for: 3 -> 0; matrix products, arithmetic and copies ran while one was open for 4% -> 0% of each run, Pallas kernels for 0% -> 0%
where the time goes in v1:
time: 109 us
  Pallas kernels  98.7 us (91%)
  local copies, waits for them, and re-layouts  9.97 us (9%)
    pallas_call x1, Pallas kernels, run_attend(): pl.pallas_call(attend_kernel, name='attend', out_shape=(jax.ShapeDtypeStr...  45.6 us
    pallas_call x1, Pallas kernels, run_project(): pl.pallas_call(project_kernel, name='project', out_shape=(jax.ShapeDtypeS...  41.8 us
    pallas_call x1, Pallas kernels, run_output(): pl.pallas_call(output_kernel, name='output', out_shape=jax.ShapeDtypeStru...  10.4 us
    unnamed x3, local copies, waits for them, and re-layouts  5.98 us

profile of v1, /device:TPU:0, one launch (start us, length us, event | category | flops | bytes accessed | tf_op | source)
XLA Modules:
  0.0 108.7 jit_solution(9662103087046309429)
XLA Ops:
  0.0 1.3 %broadcast_in_dim.16.gain = bf16[1,2048]{1,0:T(2,128)(2,1)} reshape(bf16[2048]{0:T(1024)(128)(2,1)} %param.20) | data formatting | bytes 8192 | tf_op jit(solution)/shard_map/broadcast_in_dim | solution.py:578
  1.3 1.3 %copy.20.qg = bf16[64,1]{1,0:T(8,128)(2,1)} copy(bf16[64,1]{0,1:T(2,128)(2,1)} %bitcast.11) | data formatting | bytes 256 | tf_op jit(solution)/shard_map/broadcast_in_dim | solution.py:580
  2.6 1.4 %copy.21.kg = bf16[64,1]{1,0:T(8,128)(2,1)} copy(bf16[64,1]{0,1:T(2,128)(2,1)} %bitcast.12) | data formatting | bytes 256 | tf_op jit(solution)/shard_map/broadcast_in_dim | solution.py:580
  4.0 2.0 %copy.18.wk = bf16[2048,64]{1,0:T(8,128)(2,1)} copy(bf16[2048,64]{0,1:T(8,128)(2,1)} %param.25) | data formatting | bytes 524288 | tf_op args[9]
  5.9 1.9 %copy.19.wv = bf16[2048,64]{1,0:T(8,128)(2,1)} copy(bf16[2048,64]{0,1:T(8,128)(2,1)} %param.26) | data formatting | bytes 524288 | tf_op args[10]
  7.9 41.8 %project.1 = (bf16[64,3072]{1,0:T(8,128)(2,1)}, bf16[768,128]{1,0:T(8,128)(2,1)}, bf16[512,128]{1,0:T(8,128)(2,1)}, f32[1,2048]{1,0:T(1,128)}) custom-call(bf16[192,2048]{1,0:T(8,128)(2,1)} %bitcast.7, bf16[1,128]{1,0:T(2,128)(2,1)} %cond.1, bf16[1,128]{1,0:T(2,128)(2,1)} %bitcast.10, bf16[32,2048]{1,0:T(8,128)(2,1)} %bitcast.9, ...), custom_call_target="tpu_custom_call" | custom-call | tf_op jit(solution)/shard_map/project/pallas_call | solution.py:234
  49.6 45.6 %attend.1 = (bf16[768,256]{1,0:T(8,128)(2,1)}, f32[8,3072]{1,0:T(8,128)}, bf16[16,768,128]{2,1,0:T(8,128)(2,1)}) custom-call(bf16[64,3072]{1,0:T(8,128)(2,1)} %get-tuple-element.12.q_ref.q_hbm, bf16[768,128]{1,0:T(8,128)(2,1)} %get-tuple-element.13.kv_own, bf16[512,128]{1,0:T(8,128)(2,1)} %get-tuple-element.14.ctx.ctx_hbm, f32[4]{0:T(128)} %lift.3), custom_call_target="tpu_custom_call" | custom-call | tf_op jit(solution)/shard_map/attend/pallas_call | solution.py:400
  95.2 1.0 repair.1.o_ref
  96.3 10.4 %output.1 = bf16[192,2048]{1,0:T(8,128)(2,1)} custom-call(bf16[768,256]{1,0:T(8,128)(2,1)} %repair.1.o_ref, bf16[1024,2048]{1,0:T(8,128)(2,1)} %w_hbm.1, bf16[192,2048]{1,0:T(8,128)(2,1)} %bitcast.8, f32[1,2048]{1,0:T(1,128)} %get-tuple-element.18.gate), custom_call_target="tpu_custom_call" | custom-call | tf_op jit(solution)/shard_map/output/pallas_call | solution.py:553
  106.6 2.1 %copy.24 = bf16[1,192,2048]{2,1,0:T(8,128)(2,1)} copy(bf16[1,192,2048]{2,1,0:T(8,128)(2,1)} %bitcast.6) | data formatting | bytes 1572864

commit v2 on v1

v2 whole, which is shorter than its diff:
```python
import functools

import jax
import jax.numpy as jnp
import numpy as np
from jax import lax
from jax.experimental import pallas as pl
from jax.experimental.pallas import tpu as pltpu
from jax.sharding import PartitionSpec as P

MESH = pl.DeviceIdType.MESH
HD = 64
GRID_W = 128
EPS = 1e-06
THETA = 10000.0
LOG2E = 1.4426950408889634
N_SP = 16
N_TP = 4
F32 = jnp.float32
BF16 = jnp.bfloat16
VMEM = pl.BlockSpec(memory_space=pltpu.VMEM)
ANY = pl.BlockSpec(memory_space=pl.ANY)
SMEM = pl.BlockSpec(memory_space=pltpu.SMEM)
LIMIT = 60 * 2**20


def angle_table():
    i = (np.arange(HD) // 2) % 16
    f = (THETA ** (-(i.astype(np.float32)) / np.float32(16))).astype(np.float32)
    return np.repeat(f[:, None], GRID_W, axis=1)


def tall(x):
    return jnp.concatenate([x, jnp.zeros_like(x)], axis=0)


SENDS = [
    (0, 1, 1, 0), (0, 2, -1, 0), (0, 3, 0, 1), (0, 4, 0, -1),
    (1, 5, 1, 0), (1, 6, 0, 1), (1, 7, 0, -1),
    (2, 8, 0, 1), (2, 9, 0, -1),
    (3, 10, 0, 1),
    (5, 11, 0, 1), (5, 12, 0, -1),
    (7, 13, 0, -1), (8, 14, 0, 1), (12, 15, 0, -1),
]
TILE = 1536
VROWS = 80
FIRST = 5
UNITS = 32


def attention_kernel(
    lat, cond, condc, ctx, gain, m_shift, m_scale, m_gate, wq, wk, wv, qg, kg, table, lift,
    o_out, l_out, q_out, kv_all, ctx_out, gate_out,
    xbuf, part, psum_in, mine, full, wall, ubuf, raw, cosb, sinb, scl, sft, cbuf,
    kvbuf, acc, peak, pbuf,
    x_send, x_recv, p_send, p_recv, t_send, t_recv, c_send, c_recv, kv_send, kv_recv, keep_sem,
):
    sp = lax.axis_index("sp")
    tp = lax.axis_index("tp")
    y, z = lax.rem(sp, 4), lax.div(sp, 4)
    rows, width = lat.shape
    half = rows // 2

    def sp_at(k):
        return {"sp": lax.rem(sp + k, N_SP)}

    def tp_at(k):
        return {"tp": lax.rem(tp + k, N_TP)}

    def near(dy, dz):
        return {"sp": lax.rem(z + dz + 4, 4) * 4 + lax.rem(y + dy + 4, 4)}

    barrier = pltpu.get_barrier_semaphore()
    for k in range(1, N_SP):
        pl.semaphore_signal(barrier, inc=1, device_id=sp_at(k), device_id_type=MESH)
    for k in range(1, N_TP):
        pl.semaphore_signal(barrier, inc=1, device_id=tp_at(k), device_id_type=MESH)
    pl.semaphore_wait(barrier, N_SP - 1 + N_TP - 1)

    def send(src, dst, s_sem, r_sem, target):
        return pltpu.make_async_remote_copy(
            src_ref=src, dst_ref=dst, send_sem=s_sem, recv_sem=r_sem,
            device_id=target, device_id_type=MESH,
        )

    def x_copy(i, src, to_row, count, k):
        return send(src, xbuf.at[pl.ds(to_row, count)], x_send.at[i], x_recv.at[i], tp_at(k))

    ra = x_copy(0, lat.at[pl.ds(0, 64)], 0, 64, 1)
    la = x_copy(1, lat.at[pl.ds(half, 64)], 96, 64, 3)
    rb = x_copy(2, lat.at[pl.ds(64, 32)], 64, 32, 1)
    lb = x_copy(3, lat.at[pl.ds(half + 64, 32)], 160, 32, 3)
    rc = x_copy(4, lat.at[pl.ds(half, half)], 192, half, 1)
    lc = x_copy(5, lat.at[pl.ds(0, half)], 288, half, 3)
    rf = x_copy(6, xbuf.at[pl.ds(0, half)], 384, half, 1)
    lf = x_copy(7, xbuf.at[pl.ds(half, half)], 480, half, 3)
    x_copies = [ra, la, rb, lb, rc, lc, rf, lf]
    ra.start()
    la.start()

    at = lax.broadcasted_iota(jnp.int32, (16, 128), 0)
    given = jnp.where(
        at == 0,
        jnp.broadcast_to(cond[...].astype(F32), (16, 128)),
        jnp.where(at == 1, jnp.broadcast_to(condc[...].astype(F32), (16, 128)), 0.0),
    )
    active = (given / (1.0 + jnp.exp(-given))).astype(BF16)
    for k, weight in enumerate((m_shift, m_scale, m_gate)):
        product = jnp.dot(active, weight[...], preferred_element_type=F32)
        for r in range(2):
            for c in range(4):
                i = r * 12 + k * 4 + c
                part[i : i + 1, :] = product[r : r + 1, c * 128 : (c + 1) * 128]
    p_copies = [
        send(part, psum_in.at[k - 1], p_send.at[k - 1], p_recv.at[k - 1], sp_at(k))
        for k in range(1, N_SP)
    ]
    for copy in p_copies:
        copy.start()

    wall[:, 0:256] = wq[...]
    wall[:, 256:384] = jnp.concatenate([wk[...], wv[...]], axis=0).T

    for copy in p_copies:
        copy.wait_recv()
    total = part[...]
    for k in range(N_SP - 1):
        total = total + psum_in[k]
    mine[...] = total
    full[tp] = total
    t_copies = [
        send(mine, full.at[tp], t_send.at[k - 1], t_recv.at[k - 1], tp_at(k))
        for k in range(1, N_TP)
    ]
    for copy in t_copies:
        copy.start()
    for copy in (rb, lb, rc, lc):
        copy.start()

    row_id = lax.broadcasted_iota(jnp.int32, (HD, GRID_W), 0)
    lane_id = lax.broadcasted_iota(jnp.int32, (HD, GRID_W), 1)
    even = lax.rem(row_id, 2) == 0
    left, right, opposite = (lax.rem(tp + k, N_TP) * rows for k in (3, 1, 2))
    for g in range(6):
        n = lane_id + g * 128
        shift = jnp.where(
            n < 192,
            tp * rows,
            jnp.where(
                n < 288,
                left - 192,
                jnp.where(
                    n < 384,
                    right - 192,
                    jnp.where(
                        n < 480,
                        left - 288,
                        jnp.where(n < 576, right - 480, opposite - 576),
                    ),
                ),
            ),
        )
        at_token = n + shift + sp * 768
        grid_at = jnp.where(row_id < 32, at_token >> 7, at_token & 127)
        angle = table[...] * grid_at.astype(F32)
        cosb[g] = jnp.cos(angle)
        sine = jnp.sin(angle)
        sinb[g] = jnp.where(even, -sine, sine)

    for copy in t_copies:
        copy.wait_recv()

    def vector(r, k):
        pieces = [
            full[t, r * 12 + k * 4 + c : r * 12 + k * 4 + c + 1, :]
            for t in range(N_TP)
            for c in range(4)
        ]
        return jnp.concatenate(pieces, axis=1)

    gains = gain[...].astype(F32)
    gains = jnp.concatenate([gains[i : i + 1, :] for i in range(width // 128)], axis=1)
    for r in range(2):
        scl[r] = jnp.broadcast_to(gains * (1.0 + vector(r, 1)), (8, width))
        sft[r] = jnp.broadcast_to(vector(r, 0), (8, width))
    gate_out[...] = vector(0, 2)

    def modulate(src, r, count):
        values = src.astype(F32)
        inverse = lax.rsqrt(jnp.mean(values * values, axis=-1, keepdims=True) + EPS)
        normed = (values * inverse).reshape(count // 8, 8, width)
        return (normed * scl[r][None] + sft[r][None]).reshape(count, width).astype(BF16)

    uc = modulate(ctx[...], 1, ctx.shape[0])
    craw = jnp.dot(uc, wall[:, 256:384], preferred_element_type=F32)
    lane = lax.broadcasted_iota(jnp.int32, craw.shape, 1)
    square = jnp.where(lane < HD, craw * craw, 0.0)
    mean = jnp.sum(square, axis=-1, keepdims=True) * (1.0 / HD)
    k_row = kg[...].astype(F32)
    keys = craw * lax.rsqrt(mean + EPS) * jnp.concatenate([k_row, jnp.ones((1, HD), F32)], axis=1)
    cbuf[pl.ds(0, 32), :] = jnp.where(lane < HD, keys, craw).astype(BF16)

    def project(x, first, to_row):
        @pl.loop(0, rows // 32)
        def _(i):
            at_rows = pl.ds(pl.multiple_of(i * 32, 32), 32)
            from_rows = pl.ds(pl.multiple_of(first + i * 32, 32), 32)
            ubuf[at_rows, :] = modulate(x[from_rows, :], 0, 32)

        raw[pl.ds(to_row, rows), :] = jnp.dot(ubuf[...], wall[...], preferred_element_type=F32)

    def column(ref):
        r = lax.broadcasted_iota(jnp.int32, (HD, HD), 0)
        c = lax.broadcasted_iota(jnp.int32, (HD, HD), 1)
        spread = jnp.broadcast_to(ref[...].astype(F32), (HD, HD))
        return jnp.sum(jnp.where(r == c, spread, 0.0), axis=1, keepdims=True)

    q_gain = column(qg)
    k_gain = column(kg)

    def turned(x, gain_column, g):
        square = jnp.sum(x * x, axis=0, keepdims=True) * (1.0 / HD)
        normed = x * lax.rsqrt(square + EPS) * gain_column
        up = pltpu.roll(normed, HD - 1, axis=0)
        down = pltpu.roll(normed, 1, axis=0)
        return normed * cosb[g] + jnp.where(even, up, down) * sinb[g]

    scale = LOG2E * HD ** (-0.5)

    def finish_kv(s):
        slot = s * N_SP
        for i in range(3):
            g = 3 * s + i
            side = raw[g * 128 : (g + 1) * 128, 256:384].T
            k = turned(side[0:HD], k_gain, g).T
            kvbuf[slot, i * 64 : (i + 1) * 64, :] = jnp.concatenate(
                [k[0:64], k[64:128]], axis=1
            ).astype(BF16)
        order = [(g, p) for p in range(2) for g in (3 * s, 3 * s + 1, 3 * s + 2)]
        for b in range(3):
            pieces = [
                raw[g * 128 + p * 64 : g * 128 + p * 64 + 64, 256:384]
                for g, p in order[2 * b : 2 * b + 2]
            ]
            side = jnp.concatenate(pieces, axis=0).T
            at_row = 192 + b * 64
            kvbuf[slot, at_row : at_row + 64, :] = side[HD : 2 * HD].astype(BF16)

    def finish_q(s):
        for g in range(3 * s, 3 * s + 3):
            block = raw[g * 128 : (g + 1) * 128, :]
            for pair in range(2):
                side = block[:, pair * 128 : (pair + 1) * 128].T
                for h in range(2):
                    q = turned(side[h * HD : (h + 1) * HD], q_gain, g)
                    at_lane = g * 512 + (pair * 2 + h) * 128
                    q_out[:, at_lane : at_lane + 128] = (q * scale).astype(BF16)

    kv_copies = [[], []]
    for s in range(2):
        for i, (here, there, dy, dz) in enumerate(SENDS):
            here, there = here + s * N_SP, there + s * N_SP
            kv_copies[s].append(
                send(
                    kvbuf.at[here], kvbuf.at[there],
                    kv_send.at[i + s * len(SENDS)], kv_recv.at[there], near(dy, dz),
                )
            )

    def start_from(s, slot):
        for copy, (here, _, _, _) in zip(kv_copies[s], SENDS):
            if here == slot:
                copy.start()

    def keep(s, slot):
        slot = slot + s * N_SP
        return pltpu.make_async_copy(kvbuf.at[slot], kv_all.at[slot], keep_sem.at[slot])

    def arrive(s, slot):
        if slot > 0:
            next(
                copy for copy, (_, there, _, _) in zip(kv_copies[s], SENDS) if there == slot
            ).wait_recv()
        start_from(s, slot)
        keep(s, slot).start()

    lifts = jnp.concatenate([jnp.full((1, 128), lift[h] * LOG2E, F32) for h in range(4)], axis=1)
    lifts = jnp.concatenate([lifts] * (TILE // 512), axis=1)
    ones = jnp.ones((VROWS - HD, 768), BF16)

    def lanes(t):
        if isinstance(t, int):
            return pl.ds(t * TILE, TILE)
        return pl.ds(pl.multiple_of(t * TILE, TILE), TILE)

    def context(t):
        cv = cbuf[...].astype(F32).T[HD : 2 * HD].astype(BF16)
        cv = jnp.concatenate([cv, ones[:, 0:512]], axis=0)
        scores = jnp.dot(cbuf[...], tall(q_out[:, lanes(t)]), preferred_element_type=F32) + lifts
        top = jnp.max(scores, axis=0, keepdims=True)
        peak[:, lanes(t)] = top
        weights = jnp.exp2(scores - top).astype(BF16)
        acc[:, lanes(t)] = jnp.dot(cv, weights, preferred_element_type=F32)

    def score(pair, t, slot):
        q = q_out[:, lanes(t)]
        lower = tall(q)
        upper = jnp.concatenate([jnp.zeros_like(q), q], axis=0)
        top = peak[:, lanes(t)]
        for s in range(2):
            k = kvbuf[pair * 2 + s, pl.ds(0, 192), :]
            for p, query in enumerate((lower, upper)):
                x = jnp.dot(k, query, preferred_element_type=F32)
                pbuf[slot, pl.ds(s * 384 + p * 192, 192), :] = jnp.exp2(x - top).astype(BF16)

    def value(pair, t, slot):
        v = [kvbuf[pair * 2 + s, pl.ds(192 + i * 64, 64), :] for s in range(2) for i in range(3)]
        v = jnp.concatenate([jnp.concatenate(v, axis=1), ones], axis=0)
        acc[:, lanes(t)] += jnp.dot(v, pbuf[slot], preferred_element_type=F32)

    def unit(j):
        pair = jnp.where(
            j < 10, j - FIRST, jnp.where(j < 16, 5 + (j - 10) // 2, jnp.where(j < 24, j - 8, j - 16))
        )
        tile = jnp.where(
            j < 10, 1, jnp.where(j < 16, lax.rem(j, 2), jnp.where(j < 24, 0, 1))
        )
        return pair, tile

    project(lat, 0, 0)
    c_copies = [
        send(
            cbuf.at[pl.ds(0, 32)], cbuf.at[pl.ds(32 * k, 32)],
            c_send.at[k - 1], c_recv.at[k - 1], sp_at(k),
        )
        for k in range(1, N_SP)
    ]
    for copy in c_copies:
        copy.start()
    ra.wait_recv()
    rb.wait_recv()
    rf.start()
    la.wait_recv()
    lb.wait_recv()
    lf.start()
    project(xbuf, 0, 192)
    finish_kv(0)
    finish_q(0)
    arrive(0, 0)
    for copy in c_copies:
        copy.wait_recv()
    context(0)
    arrive(0, 1)
    score(0, 0, 0)

    def first_step(j, carry):
        for pair in range(1, FIRST):

            @pl.when(j == pair - 1)
            def _(pair=pair):
                arrive(0, 2 * pair)
                arrive(0, 2 * pair + 1)

        slot = lax.rem(j, 2)
        value(j, 0, slot)
        score(j + 1, 0, 1 - slot)
        return carry

    lax.fori_loop(0, FIRST - 1, first_step, 0)
    value(FIRST - 1, 0, (FIRST - 1) % 2)

    rc.wait_recv()
    lc.wait_recv()
    project(xbuf, 192, 384)
    rf.wait_recv()
    lf.wait_recv()
    project(xbuf, 384, 576)
    finish_kv(1)
    finish_q(1)
    arrive(1, 0)
    context(1)
    score(0, 1, FIRST % 2)

    events = {5: (0, 5), 6: (0, 6), 7: (0, 7)}
    for pair, j in enumerate((9, 10, 11, 12, 13, 14, 16, 18)):
        events[j] = (1, pair)

    def second_step(j, carry):
        for when, (s, pair) in events.items():

            @pl.when(j == when)
            def _(s=s, pair=pair):
                for slot in (2 * pair, 2 * pair + 1):
                    if slot > 0:
                        arrive(s, slot)

        slot = lax.rem(j, 2)
        value(*unit(j), slot)
        score(*unit(j + 1), 1 - slot)
        return carry

    lax.fori_loop(FIRST, UNITS - 1, second_step, 0)
    value(15, 1, (UNITS - 1) % 2)

    l_out[...] = acc[HD : HD + 8, :]
    for g in range(6):
        at_lanes = pl.ds(g * 512, 512)
        mean = acc[0:HD, at_lanes] / acc[HD : HD + 1, at_lanes]
        stack = jnp.concatenate([mean[:, h * 128 : (h + 1) * 128] for h in range(4)], axis=0)
        o_out[g * 128 : (g + 1) * 128, :] = stack.T.astype(BF16)
    ctx_out[...] = cbuf[...]
    for copy in x_copies + p_copies + t_copies + c_copies + kv_copies[0] + kv_copies[1]:
        copy.wait_send()
    for s in range(2):
        for slot in range(N_SP):
            keep(s, slot).wait()


def run_attention(lat, cond, condc, ctx, gain, ms, mc, mg, wq, wk, wv, qg, kg, lift):
    rows, width = lat.shape
    dma = pltpu.SemaphoreType.DMA
    return pl.pallas_call(
        attention_kernel,
        name="attention",
        out_shape=(
            jax.ShapeDtypeStruct((768, 256), BF16),
            jax.ShapeDtypeStruct((8, 3072), F32),
            jax.ShapeDtypeStruct((HD, 3072), BF16),
            jax.ShapeDtypeStruct((2 * N_SP, 384, 128), BF16),
            jax.ShapeDtypeStruct((512, 128), BF16),
            jax.ShapeDtypeStruct((1, width), F32),
        ),
        in_specs=[VMEM] * 14 + [SMEM],
        out_specs=(VMEM, VMEM, VMEM, ANY, VMEM, VMEM),
        scratch_shapes=[
            pltpu.VMEM((3 * rows, width), BF16),
            pltpu.VMEM((24, 128), F32),
            pltpu.VMEM((N_SP - 1, 24, 128), F32),
            pltpu.VMEM((24, 128), F32),
            pltpu.VMEM((N_TP, 24, 128), F32),
            pltpu.VMEM((width, 384), BF16),
            pltpu.VMEM((rows, width), BF16),
            pltpu.VMEM((768, 384), F32),
            pltpu.VMEM((6, HD, GRID_W), F32),
            pltpu.VMEM((6, HD, GRID_W), F32),
            pltpu.VMEM((2, 8, width), F32),
            pltpu.VMEM((2, 8, width), F32),
            pltpu.VMEM((512, 128), BF16),
            pltpu.VMEM((2 * N_SP, 384, 128), BF16),
            pltpu.VMEM((VROWS, 3072), F32),
            pltpu.VMEM((1, 3072), F32),
            pltpu.VMEM((2, 768, TILE), BF16),
            dma((8,)), dma((8,)), dma((15,)), dma((15,)),
            dma((3,)), dma((3,)), dma((15,)), dma((15,)),
            dma((2 * len(SENDS),)), dma((2 * N_SP,)), dma((2 * N_SP,)),
        ],
        compiler_params=pltpu.CompilerParams(
            collective_id=0, has_side_effects=True, vmem_limit_bytes=LIMIT
        ),
    )(
        lat, cond, condc, ctx, gain, ms, mc, mg, wq, wk, wv, qg, kg,
        jnp.asarray(angle_table()), lift,
    )


def repair_kernel(
    l_ref, o_in, q_hbm, kv_hbm, ctx_hbm, lift, o_out,
    q_ref, kvbuf, ctx, acc, peak, o_buf, sem,
):
    safe = jnp.all(l_ref[...] < 2.0**100)

    @pl.when(jnp.logical_not(safe))
    def _():
        for src, dst in ((q_hbm, q_ref), (kv_hbm, kvbuf), (ctx_hbm, ctx)):
            copy = pltpu.make_async_copy(src, dst, sem)
            copy.start()
            copy.wait()
        wide = 512
        ones = jnp.ones((VROWS - HD, 768), BF16)
        lifts = jnp.concatenate(
            [jnp.full((1, 128), lift[h] * LOG2E, F32) for h in range(4)], axis=1
        )
        cv = ctx[...].astype(F32).T[HD : 2 * HD].astype(BF16)
        cv = jnp.concatenate([cv, ones[:, 0:512]], axis=0)

        @pl.loop(0, q_ref.shape[1] // wide)
        def _(t):
            lanes = pl.ds(pl.multiple_of(t * wide, wide), wide)
            q = q_ref[:, lanes]
            left = tall(q)
            right = jnp.concatenate([jnp.zeros_like(q), q], axis=0)
            scores = jnp.dot(ctx[...], left, preferred_element_type=F32) + lifts
            top = jnp.max(scores, axis=0, keepdims=True)
            peak[...] = top
            weights = jnp.exp2(scores - top).astype(BF16)
            acc[...] = jnp.dot(cv, weights, preferred_element_type=F32)

            @pl.loop(0, N_SP)
            def _(b):
                parts = []
                for s in range(2):
                    k = kvbuf[b * 2 + s, pl.ds(0, 192), :]
                    for query in (left, right):
                        parts.append(jnp.dot(k, query, preferred_element_type=F32))
                x = jnp.concatenate(parts, axis=0)
                old = peak[...]
                new = jnp.maximum(old, jnp.max(x, axis=0, keepdims=True))
                peak[...] = new
                v = [
                    kvbuf[b * 2 + s, pl.ds(192 + i * 64, 64), :] for s in range(2) for i in range(3)
                ]
                v = jnp.concatenate([jnp.concatenate(v, axis=1), ones], axis=0)
                weights = jnp.exp2(x - new).astype(BF16)
                acc[...] = acc[...] * jnp.exp2(old - new) + jnp.dot(
                    v, weights, preferred_element_type=F32
                )

            mean = acc[0:HD, :] / acc[HD : HD + 1, :]
            stack = jnp.concatenate([mean[:, h * 128 : (h + 1) * 128] for h in range(4)], axis=0)
            o_buf[...] = stack.T.astype(BF16)
            rows = pl.ds(pl.multiple_of(t * 128, 128), 128)
            copy = pltpu.make_async_copy(o_buf, o_out.at[rows], sem)
            copy.start()
            copy.wait()


def run_repair(l, o, q, kv_all, ctx, lift):
    return pl.pallas_call(
        repair_kernel,
        name="repair",
        out_shape=jax.ShapeDtypeStruct(o.shape, o.dtype),
        in_specs=[VMEM, ANY, ANY, ANY, ANY, SMEM],
        out_specs=ANY,
        input_output_aliases={1: 0},
        scratch_shapes=[
            pltpu.VMEM((HD, 3072), BF16),
            pltpu.VMEM((2 * N_SP, 384, 128), BF16),
            pltpu.VMEM((512, 128), BF16),
            pltpu.VMEM((VROWS, 512), F32),
            pltpu.VMEM((1, 512), F32),
            pltpu.VMEM((128, 256), BF16),
            pltpu.SemaphoreType.DMA(()),
        ],
        compiler_params=pltpu.CompilerParams(vmem_limit_bytes=LIMIT),
    )(l, o, q, kv_all, ctx, lift)


def exchange_kernel(o_ref, out, obuf, send_sem, recv_sem):
    tp = lax.axis_index("tp")
    rows = o_ref.shape[0] // N_TP
    half = rows // 2

    def tp_at(k):
        return {"tp": lax.rem(tp + k, N_TP)}

    barrier = pltpu.get_barrier_semaphore()
    for k in range(1, N_TP):
        pl.semaphore_signal(barrier, inc=1, device_id=tp_at(k), device_id_type=MESH)
    pl.semaphore_wait(barrier, N_TP - 1)
    plan = [(2, 576, 0, rows), (3, 192, 0, half), (1, 288, half, half), (3, 384, half, half),
            (1, 480, 0, half)]
    copies = []
    for i, (k, here, there, count) in enumerate(plan):
        copies.append(
            pltpu.make_async_remote_copy(
                src_ref=o_ref.at[pl.ds(here, count)],
                dst_ref=obuf.at[tp, pl.ds(there, count)],
                send_sem=send_sem.at[i], recv_sem=recv_sem.at[i],
                device_id=tp_at(k), device_id_type=MESH,
            )
        )
        copies[-1].start()
    out[tp] = o_ref[0:rows, :]
    for copy in copies:
        copy.wait_recv()
    for k in range(1, N_TP):
        source = lax.rem(tp + k, N_TP)
        out[source] = obuf[source]
    for copy in copies:
        copy.wait_send()


def run_exchange(o):
    rows = o.shape[0] // N_TP
    dma = pltpu.SemaphoreType.DMA
    return pl.pallas_call(
        exchange_kernel,
        name="exchange",
        out_shape=jax.ShapeDtypeStruct((N_TP, rows, 256), BF16),
        in_specs=[VMEM],
        out_specs=VMEM,
        scratch_shapes=[pltpu.VMEM((N_TP, rows, 256), BF16), dma((5,)), dma((5,))],
        compiler_params=pltpu.CompilerParams(collective_id=2, has_side_effects=True),
    )(o)


def output_kernel(o_ref, w, lat, gate, out):
    total = None
    for t in range(N_TP):
        term = jnp.dot(o_ref[t], w[t * 256 : (t + 1) * 256, :], preferred_element_type=F32)
        total = term if total is None else total + term
    out[...] = (lat[...].astype(F32) + gate[...] * total).astype(BF16)


def run_output(o, w_out, lat, gate):
    rows, width = lat.shape
    wide = 512
    return pl.pallas_call(
        output_kernel,
        name="output",
        grid=(width // wide,),
        out_shape=jax.ShapeDtypeStruct((rows, width), BF16),
        in_specs=[
            pl.BlockSpec((N_TP, rows, 256), lambda n: (0, 0, 0)),
            pl.BlockSpec((w_out.shape[0], wide), lambda n: (0, n)),
            pl.BlockSpec((rows, wide), lambda n: (0, n)),
            pl.BlockSpec((1, wide), lambda n: (0, n)),
        ],
        out_specs=pl.BlockSpec((rows, wide), lambda n: (0, n)),
    )(o, w_out, lat, gate)


def on_device(
    latent, cond, cond_ctx, context, norm_gain, mod_shift, mod_scale, mod_gate,
    w_query, w_key, w_value, q_gain, k_gain, ctx_lift, w_out,
):
    lat = latent[0]
    o, l, q, kv_all, ctx, gate = run_attention(
        lat, cond, cond_ctx[None, :], context[0], norm_gain.reshape(-1, 128),
        mod_shift, mod_scale, mod_gate, w_query, w_key.T, w_value.T,
        q_gain[None, :], k_gain[None, :], ctx_lift,
    )
    o = run_repair(l, o, q, kv_all, ctx, ctx_lift)
    return run_output(run_exchange(o), w_out, lat, gate)[None]


def solution(mesh):
    in_specs = (
        P("dp", ("sp", "tp"), None),
        P("dp", "sp"),
        P("sp"),
        P("dp", "sp", None),
        P(),
        P("sp", "tp"),
        P("sp", "tp"),
        P("sp", "tp"),
        P(None, "tp"),
        P(None, "tp"),
        P(None, "tp"),
        P(),
        P(),
        P("tp"),
        P(),
    )
    return jax.shard_map(
        on_device, mesh=mesh, in_specs=in_specs,
        out_specs=P("dp", ("sp", "tp"), None), check_vma=False,
    )
```

time: 109 us -> 98.7 us (0.906)
  local copies, waits for them, and re-layouts: 9.97 us -> 0 us
    unnamed x3 -> x0, local copies, waits for them, and re-layouts: 5.98 us -> none
    broadcast_in_dim x3 -> x0, local copies, waits for them, and re-layouts: 3.99 us -> none  [the longest x1 1.35 us: on_device(): k_gain[:, None]]
where the time goes in v2:
time: 98.7 us; the launch traced here: 98.4 us
  Pallas kernels  98.3 us (100%)
    pallas_call x1, Pallas kernels, run_attention(): pl.pallas_call(attention_kernel, name='attention', out_shape=(jax.ShapeDt...  83.6 us
    pallas_call x1, Pallas kernels, run_exchange(): pl.pallas_call(exchange_kernel, name='exchange', out_shape=jax.ShapeDtype...  8.73 us
    pallas_call x1, Pallas kernels, run_output(): pl.pallas_call(output_kernel, name='output', grid=(width // wide,), out_s...  5.01 us

profile of v2, /device:TPU:0, one launch (start us, length us, event | category | flops | bytes accessed | tf_op | source)
XLA Modules:
  0.0 98.4 jit_solution(2271351142096374069)
XLA Ops:
  0.0 83.6 %attention.1 = (bf16[768,256]{1,0:T(8,128)(2,1)}, f32[8,3072]{1,0:T(8,128)}, bf16[64,3072]{1,0:T(8,128)(2,1)}, bf16[32,384,128]{2,1,0:T(8,128)(2,1)}, bf16[512,128]{1,0:T(8,128)(2,1)}, /*index=5*/f32[1,2048]{1,0:T(1,128)}) custom-call(bf16[192,2048]{1,0:T(8,128)(2,1)} %bitcast.9, bf16[1,128]{1,0:T(2,128)(2,1)} %cond.1, bf16[1,128]{1,0:T(2,128)(2,1)} %bitcast.15, ...), custom_call_target="tpu_custom_call" | custom-call | tf_op jit(solution)/shard_map/attention/pallas_call | solution.py:422
  83.6 1.0 %repair.1.o_ref = bf16[768,256]{1,0:T(8,128)(2,1)} custom-call(f32[8,3072]{1,0:T(8,128)} %get-tuple-element.11.l_ref, bf16[768,256]{1,0:T(8,128)(2,1)} %get-tuple-element.12.o_in, bf16[64,3072]{1,0:T(8,128)(2,1)} %get-tuple-element.13.q_hbm, bf16[32,384,128]{2,1,0:T(8,128)(2,1)} %get-tuple-element.14.kv_hbm, ...), custom_call_target="tpu_custom_call", output_to_operand_aliasing={{}: (1, {})} | custom-call | tf_op jit(solution)/shard_map/repair/pallas_call | solution.py:528
  84.6 8.7 %exchange.1.o_ref = bf16[4,192,256]{2,1,0:T(8,128)(2,1)} custom-call(bf16[768,256]{1,0:T(8,128)(2,1)} %repair.1.o_ref), custom_call_target="tpu_custom_call" | custom-call | tf_op jit(solution)/shard_map/exchange/pallas_call | solution.py:586
  93.4 5.0 %output.1 = bf16[192,2048]{1,0:T(8,128)(2,1)} custom-call(bf16[4,192,256]{2,1,0:T(8,128)(2,1)} %exchange.1.o_ref, bf16[1024,2048]{1,0:T(8,128)(2,1)} %w.1, bf16[192,2048]{1,0:T(8,128)(2,1)} %bitcast.10, f32[1,2048]{1,0:T(1,128)} %get-tuple-element.16.gate), custom_call_target="tpu_custom_call" | custom-call | tf_op jit(solution)/shard_map/output/pallas_call | solution.py:608

commit v3 on v2

--- a/solution.py
+++ b/solution.py
@@ -19,9 +19,8 @@
 F32 = jnp.float32
 BF16 = jnp.bfloat16
 VMEM = pl.BlockSpec(memory_space=pltpu.VMEM)
-ANY = pl.BlockSpec(memory_space=pl.ANY)
+HBM = pl.BlockSpec(memory_space=pltpu.HBM)
 SMEM = pl.BlockSpec(memory_space=pltpu.SMEM)
-LIMIT = 60 * 2**20
 
 
 def angle_table():
@@ -43,16 +42,18 @@
     (7, 13, 0, -1), (8, 14, 0, 1), (12, 15, 0, -1),
 ]
 TILE = 1536
+NARROW = 512
 VROWS = 80
 FIRST = 5
 UNITS = 32
 
 
 def attention_kernel(
-    lat, cond, condc, ctx, gain, m_shift, m_scale, m_gate, wq, wk, wv, qg, kg, table, lift,
-    o_out, l_out, q_out, kv_all, ctx_out, gate_out,
+    lat_hbm, ctx_hbm, ms_hbm, mc_hbm, mg_hbm, wq_hbm, wk_hbm, wv_hbm,
+    cond, condc, gain, qg, kg, table, lift,
+    o_out, l_out, q_all, kv_all, ctx_all, gate_out,
     xbuf, part, psum_in, mine, full, wall, ubuf, raw, cosb, sinb, scl, sft, cbuf,
-    kvbuf, acc, peak, pbuf,
+    q_out, kvbuf, acc, peak, p_even, p_odd, lat, ctx, m_shift, m_scale, m_gate, wq, wk, wv, load_sem,
     x_send, x_recv, p_send, p_recv, t_send, t_recv, c_send, c_recv, kv_send, kv_recv, keep_sem,
 ):
     sp = lax.axis_index("sp")
@@ -75,6 +76,13 @@
         pl.semaphore_signal(barrier, inc=1, device_id=sp_at(k), device_id_type=MESH)
     for k in range(1, N_TP):
         pl.semaphore_signal(barrier, inc=1, device_id=tp_at(k), device_id_type=MESH)
+    pairs = zip(
+        (ms_hbm, mc_hbm, mg_hbm, lat_hbm, ctx_hbm, wq_hbm, wk_hbm, wv_hbm),
+        (m_shift, m_scale, m_gate, lat, ctx, wq, wk, wv),
+    )
+    loads = [pltpu.make_async_copy(a, b, load_sem.at[i]) for i, (a, b) in enumerate(pairs)]
+    for load in loads:
+        load.start()
     pl.semaphore_wait(barrier, N_SP - 1 + N_TP - 1)
 
     def send(src, dst, s_sem, r_sem, target):
@@ -86,12 +94,12 @@
     def x_copy(i, src, to_row, count, k):
         return send(src, xbuf.at[pl.ds(to_row, count)], x_send.at[i], x_recv.at[i], tp_at(k))
 
-    ra = x_copy(0, lat.at[pl.ds(0, 64)], 0, 64, 1)
-    la = x_copy(1, lat.at[pl.ds(half, 64)], 96, 64, 3)
-    rb = x_copy(2, lat.at[pl.ds(64, 32)], 64, 32, 1)
-    lb = x_copy(3, lat.at[pl.ds(half + 64, 32)], 160, 32, 3)
-    rc = x_copy(4, lat.at[pl.ds(half, half)], 192, half, 1)
-    lc = x_copy(5, lat.at[pl.ds(0, half)], 288, half, 3)
+    ra = x_copy(0, lat_hbm.at[pl.ds(0, 64)], 0, 64, 1)
+    la = x_copy(1, lat_hbm.at[pl.ds(half, 64)], 96, 64, 3)
+    rb = x_copy(2, lat_hbm.at[pl.ds(64, 32)], 64, 32, 1)
+    lb = x_copy(3, lat_hbm.at[pl.ds(half + 64, 32)], 160, 32, 3)
+    rc = x_copy(4, lat_hbm.at[pl.ds(half, half)], 192, half, 1)
+    lc = x_copy(5, lat_hbm.at[pl.ds(0, half)], 288, half, 3)
     rf = x_copy(6, xbuf.at[pl.ds(0, half)], 384, half, 1)
     lf = x_copy(7, xbuf.at[pl.ds(half, half)], 480, half, 3)
     x_copies = [ra, la, rb, lb, rc, lc, rf, lf]
@@ -104,6 +112,8 @@
         jnp.broadcast_to(cond[...].astype(F32), (16, 128)),
         jnp.where(at == 1, jnp.broadcast_to(condc[...].astype(F32), (16, 128)), 0.0),
     )
+    for load in loads[0:3]:
+        load.wait()
     active = (given / (1.0 + jnp.exp(-given))).astype(BF16)
     for k, weight in enumerate((m_shift, m_scale, m_gate)):
         product = jnp.dot(active, weight[...], preferred_element_type=F32)
@@ -118,6 +128,8 @@
     for copy in p_copies:
         copy.start()
 
+    for load in loads[3:]:
+        load.wait()
     wall[:, 0:256] = wq[...]
     wall[:, 256:384] = jnp.concatenate([wk[...], wv[...]], axis=0).T
 
@@ -200,13 +212,15 @@
     keys = craw * lax.rsqrt(mean + EPS) * jnp.concatenate([k_row, jnp.ones((1, HD), F32)], axis=1)
     cbuf[pl.ds(0, 32), :] = jnp.where(lane < HD, keys, craw).astype(BF16)
 
-    def project(x, first, to_row):
+    def project(x, first, to_row, between=None):
         @pl.loop(0, rows // 32)
         def _(i):
             at_rows = pl.ds(pl.multiple_of(i * 32, 32), 32)
             from_rows = pl.ds(pl.multiple_of(first + i * 32, 32), 32)
             ubuf[at_rows, :] = modulate(x[from_rows, :], 0, 32)
 
+        if between is not None:
+            between()
         raw[pl.ds(to_row, rows), :] = jnp.dot(ubuf[...], wall[...], preferred_element_type=F32)
 
     def column(ref):
@@ -246,8 +260,8 @@
             at_row = 192 + b * 64
             kvbuf[slot, at_row : at_row + 64, :] = side[HD : 2 * HD].astype(BF16)
 
-    def finish_q(s):
-        for g in range(3 * s, 3 * s + 3):
+    def finish_q(blocks):
+        for g in blocks:
             block = raw[g * 128 : (g + 1) * 128, :]
             for pair in range(2):
                 side = block[:, pair * 128 : (pair + 1) * 128].T
@@ -293,6 +307,10 @@
             return pl.ds(t * TILE, TILE)
         return pl.ds(pl.multiple_of(t * TILE, TILE), TILE)
 
+    def narrow(t, n):
+        start = t * TILE + n * NARROW
+        return pl.ds(start if isinstance(t, int) else pl.multiple_of(start, NARROW), NARROW)
+
     def context(t):
         cv = cbuf[...].astype(F32).T[HD : 2 * HD].astype(BF16)
         cv = jnp.concatenate([cv, ones[:, 0:512]], axis=0)
@@ -302,32 +320,52 @@
         weights = jnp.exp2(scores - top).astype(BF16)
         acc[:, lanes(t)] = jnp.dot(cv, weights, preferred_element_type=F32)
 
-    def score(pair, t, slot):
-        q = q_out[:, lanes(t)]
-        lower = tall(q)
-        upper = jnp.concatenate([jnp.zeros_like(q), q], axis=0)
-        top = peak[:, lanes(t)]
-        for s in range(2):
-            k = kvbuf[pair * 2 + s, pl.ds(0, 192), :]
-            for p, query in enumerate((lower, upper)):
-                x = jnp.dot(k, query, preferred_element_type=F32)
-                pbuf[slot, pl.ds(s * 384 + p * 192, 192), :] = jnp.exp2(x - top).astype(BF16)
-
-    def value(pair, t, slot):
+    def query_forms(at_lanes):
+        q = q_out[:, at_lanes]
+        return tall(q), jnp.concatenate([jnp.zeros_like(q), q], axis=0)
+
+    def values_of(pair):
         v = [kvbuf[pair * 2 + s, pl.ds(192 + i * 64, 64), :] for s in range(2) for i in range(3)]
-        v = jnp.concatenate([jnp.concatenate(v, axis=1), ones], axis=0)
-        acc[:, lanes(t)] += jnp.dot(v, pbuf[slot], preferred_element_type=F32)
+        return jnp.concatenate([jnp.concatenate(v, axis=1), ones], axis=0)
+
+    def work(now, then, read, write):
+        if now is not None:
+            v = values_of(now[0])
+        for n in range(TILE // NARROW):
+            cols = slice(n * NARROW, (n + 1) * NARROW)
+            if then is not None:
+                theirs = narrow(then[1], n)
+                forms = query_forms(theirs)
+                top = peak[:, theirs]
+            total = None
+            for i in range(4):
+                if then is not None:
+                    s, p = i % 2, i // 2
+                    k = kvbuf[then[0] * 2 + s, pl.ds(0, 192), :]
+                    x = jnp.dot(k, forms[p], preferred_element_type=F32)
+                    write[pl.ds(s * 384 + p * 192, 192), cols] = jnp.exp2(x - top).astype(BF16)
+                if now is not None and i < 3:
+                    term = jnp.dot(
+                        v[:, i * 256 : (i + 1) * 256], read[pl.ds(i * 256, 256), cols],
+                        preferred_element_type=F32,
+                    )
+                    total = term if total is None else total + term
+            if now is not None:
+                acc[:, narrow(now[1], n)] += total
 
     def unit(j):
         pair = jnp.where(
-            j < 10, j - FIRST, jnp.where(j < 16, 5 + (j - 10) // 2, jnp.where(j < 24, j - 8, j - 16))
+            j < 2 * FIRST,
+            j - FIRST,
+            jnp.where(
+                j < 16, FIRST + (j - 2 * FIRST) // 2, jnp.where(j < 24, j - 8, j - 16)
+            ),
         )
         tile = jnp.where(
-            j < 10, 1, jnp.where(j < 16, lax.rem(j, 2), jnp.where(j < 24, 0, 1))
+            j < 2 * FIRST, 1, jnp.where(j < 16, lax.rem(j, 2), jnp.where(j < 24, 0, 1))
         )
         return pair, tile
 
-    project(lat, 0, 0)
     c_copies = [
         send(
             cbuf.at[pl.ds(0, 32)], cbuf.at[pl.ds(32 * k, 32)],
@@ -335,8 +373,12 @@
         )
         for k in range(1, N_SP)
     ]
-    for copy in c_copies:
-        copy.start()
+
+    def start_context():
+        for copy in c_copies:
+            copy.start()
+
+    project(lat, 0, 0, start_context)
     ra.wait_recv()
     rb.wait_recv()
     rf.start()
@@ -345,29 +387,29 @@
     lf.start()
     project(xbuf, 0, 192)
     finish_kv(0)
-    finish_q(0)
+    finish_q((0,))
     arrive(0, 0)
+    finish_q((1, 2))
     for copy in c_copies:
         copy.wait_recv()
     context(0)
     arrive(0, 1)
-    score(0, 0, 0)
-
-    def first_step(j, carry):
+    work(None, (0, 0), None, p_even)
+
+    def first_step(d, carry):
         for pair in range(1, FIRST):
 
-            @pl.when(j == pair - 1)
+            @pl.when(d == (pair - 1) // 2)
             def _(pair=pair):
                 arrive(0, 2 * pair)
                 arrive(0, 2 * pair + 1)
 
-        slot = lax.rem(j, 2)
-        value(j, 0, slot)
-        score(j + 1, 0, 1 - slot)
+        work((2 * d, 0), (2 * d + 1, 0), p_even, p_odd)
+        work((2 * d + 1, 0), (2 * d + 2, 0), p_odd, p_even)
         return carry
 
-    lax.fori_loop(0, FIRST - 1, first_step, 0)
-    value(FIRST - 1, 0, (FIRST - 1) % 2)
+    lax.fori_loop(0, FIRST // 2, first_step, 0)
+    work((FIRST - 1, 0), None, p_even, None)
 
     rc.wait_recv()
     lc.wait_recv()
@@ -376,31 +418,38 @@
     lf.wait_recv()
     project(xbuf, 384, 576)
     finish_kv(1)
-    finish_q(1)
+    finish_q((3,))
     arrive(1, 0)
+    finish_q((4, 5))
     context(1)
-    score(0, 1, FIRST % 2)
-
-    events = {5: (0, 5), 6: (0, 6), 7: (0, 7)}
-    for pair, j in enumerate((9, 10, 11, 12, 13, 14, 16, 18)):
-        events[j] = (1, pair)
-
-    def second_step(j, carry):
-        for when, (s, pair) in events.items():
-
-            @pl.when(j == when)
-            def _(s=s, pair=pair):
-                for slot in (2 * pair, 2 * pair + 1):
-                    if slot > 0:
-                        arrive(s, slot)
-
-        slot = lax.rem(j, 2)
-        value(*unit(j), slot)
-        score(*unit(j + 1), 1 - slot)
+    keep_rest = [
+        pltpu.make_async_copy(q_out, q_all, keep_sem.at[2 * N_SP]),
+        pltpu.make_async_copy(cbuf, ctx_all, keep_sem.at[2 * N_SP + 1]),
+    ]
+    for copy in keep_rest:
+        copy.start()
+    work(None, (0, 1), None, p_even)
+
+    events = [(0, 0, (5,)), (1, 0, (6,)), (2, 1, (0, 1)), (3, 0, (7,)), (3, 1, (2, 3)),
+              (4, 1, (4,)), (5, 1, (5,)), (6, 1, (6,)), (8, 1, (7,))]
+
+    def second_step(d, carry):
+        for when, s, pairs in events:
+
+            @pl.when(d == when)
+            def _(s=s, pairs=pairs):
+                for pair in pairs:
+                    for slot in (2 * pair, 2 * pair + 1):
+                        if slot > 0:
+                            arrive(s, slot)
+
+        j = FIRST + 2 * d
+        work(unit(j), unit(j + 1), p_even, p_odd)
+        work(unit(j + 1), unit(j + 2), p_odd, p_even)
         return carry
 
-    lax.fori_loop(FIRST, UNITS - 1, second_step, 0)
-    value(15, 1, (UNITS - 1) % 2)
+    lax.fori_loop(0, (UNITS - 1 - FIRST) // 2, second_step, 0)
+    work((15, 1), None, p_even, None)
 
     l_out[...] = acc[HD : HD + 8, :]
     for g in range(6):
@@ -408,17 +457,19 @@
         mean = acc[0:HD, at_lanes] / acc[HD : HD + 1, at_lanes]
         stack = jnp.concatenate([mean[:, h * 128 : (h + 1) * 128] for h in range(4)], axis=0)
         o_out[g * 128 : (g + 1) * 128, :] = stack.T.astype(BF16)
-    ctx_out[...] = cbuf[...]
     for copy in x_copies + p_copies + t_copies + c_copies + kv_copies[0] + kv_copies[1]:
         copy.wait_send()
     for s in range(2):
         for slot in range(N_SP):
             keep(s, slot).wait()
+    for copy in keep_rest:
+        copy.wait()
 
 
 def run_attention(lat, cond, condc, ctx, gain, ms, mc, mg, wq, wk, wv, qg, kg, lift):
     rows, width = lat.shape
     dma = pltpu.SemaphoreType.DMA
+    loaded = (lat, ctx, ms, mc, mg, wq, wk, wv)
     return pl.pallas_call(
         attention_kernel,
         name="attention",
@@ -430,8 +481,8 @@
             jax.ShapeDtypeStruct((512, 128), BF16),
             jax.ShapeDtypeStruct((1, width), F32),
         ),
-        in_specs=[VMEM] * 14 + [SMEM],
-        out_specs=(VMEM, VMEM, VMEM, ANY, VMEM, VMEM),
+        in_specs=[HBM] * 8 + [VMEM] * 6 + [SMEM],
+        out_specs=(VMEM, VMEM, HBM, HBM, HBM, VMEM),
         scratch_shapes=[
             pltpu.VMEM((3 * rows, width), BF16),
             pltpu.VMEM((24, 128), F32),
@@ -446,28 +497,35 @@
             pltpu.VMEM((2, 8, width), F32),
             pltpu.VMEM((2, 8, width), F32),
             pltpu.VMEM((512, 128), BF16),
+            pltpu.VMEM((HD, 3072), BF16),
             pltpu.VMEM((2 * N_SP, 384, 128), BF16),
             pltpu.VMEM((VROWS, 3072), F32),
             pltpu.VMEM((1, 3072), F32),
-            pltpu.VMEM((2, 768, TILE), BF16),
+            pltpu.VMEM((768, TILE), BF16),
+            pltpu.VMEM((768, TILE), BF16),
+            *[pltpu.VMEM(a.shape, BF16) for a in loaded],
+            dma((len(loaded),)),
             dma((8,)), dma((8,)), dma((15,)), dma((15,)),
             dma((3,)), dma((3,)), dma((15,)), dma((15,)),
-            dma((2 * len(SENDS),)), dma((2 * N_SP,)), dma((2 * N_SP,)),
+            dma((2 * len(SENDS),)), dma((2 * N_SP,)), dma((2 * N_SP + 2,)),
         ],
         compiler_params=pltpu.CompilerParams(
-            collective_id=0, has_side_effects=True, vmem_limit_bytes=LIMIT
+            collective_id=0, has_side_effects=True, vmem_limit_bytes=60 * 2**20
+        ),
+        cost_estimate=pl.CostEstimate(
+            flops=2 * 10**10, bytes_accessed=10**7, transcendentals=4 * 10**7
         ),
     )(
-        lat, cond, condc, ctx, gain, ms, mc, mg, wq, wk, wv, qg, kg,
-        jnp.asarray(angle_table()), lift,
+        *loaded, cond, condc, gain, qg, kg, jnp.asarray(angle_table()), lift,
     )
 
 
 def repair_kernel(
     l_ref, o_in, q_hbm, kv_hbm, ctx_hbm, lift, o_out,
-    q_ref, kvbuf, ctx, acc, peak, o_buf, sem,
+    q_ref, kvbuf, ctx, acc, peak, sem,
 ):
     safe = jnp.all(l_ref[...] < 2.0**100)
+    o_out[...] = o_in[...]
 
     @pl.when(jnp.logical_not(safe))
     def _():
@@ -517,11 +575,8 @@
 
             mean = acc[0:HD, :] / acc[HD : HD + 1, :]
             stack = jnp.concatenate([mean[:, h * 128 : (h + 1) * 128] for h in range(4)], axis=0)
-            o_buf[...] = stack.T.astype(BF16)
             rows = pl.ds(pl.multiple_of(t * 128, 128), 128)
-            copy = pltpu.make_async_copy(o_buf, o_out.at[rows], sem)
-            copy.start()
-            copy.wait()
+            o_out[rows, :] = stack.T.astype(BF16)
 
 
 def run_repair(l, o, q, kv_all, ctx, lift):
@@ -529,19 +584,17 @@
         repair_kernel,
         name="repair",
         out_shape=jax.ShapeDtypeStruct(o.shape, o.dtype),
-        in_specs=[VMEM, ANY, ANY, ANY, ANY, SMEM],
-        out_specs=ANY,
-        input_output_aliases={1: 0},
+        in_specs=[VMEM, VMEM, HBM, HBM, HBM, SMEM],
+        out_specs=VMEM,
         scratch_shapes=[
             pltpu.VMEM((HD, 3072), BF16),
             pltpu.VMEM((2 * N_SP, 384, 128), BF16),
             pltpu.VMEM((512, 128), BF16),
             pltpu.VMEM((VROWS, 512), F32),
             pltpu.VMEM((1, 512), F32),
-            pltpu.VMEM((128, 256), BF16),
             pltpu.SemaphoreType.DMA(()),
         ],
-        compiler_params=pltpu.CompilerParams(vmem_limit_bytes=LIMIT),
+        compiler_params=pltpu.CompilerParams(vmem_limit_bytes=60 * 2**20),
     )(l, o, q, kv_all, ctx, lift)
 
 
@@ -590,33 +643,34 @@
         in_specs=[VMEM],
         out_specs=VMEM,
         scratch_shapes=[pltpu.VMEM((N_TP, rows, 256), BF16), dma((5,)), dma((5,))],
-        compiler_params=pltpu.CompilerParams(collective_id=2, has_side_effects=True),
+        compiler_params=pltpu.CompilerParams(
+            collective_id=2, has_side_effects=True, vmem_limit_bytes=4 * 2**20
+        ),
+        cost_estimate=pl.CostEstimate(flops=0, bytes_accessed=25 * 10**6, transcendentals=0),
     )(o)
 
 
 def output_kernel(o_ref, w, lat, gate, out):
-    total = None
-    for t in range(N_TP):
-        term = jnp.dot(o_ref[t], w[t * 256 : (t + 1) * 256, :], preferred_element_type=F32)
-        total = term if total is None else total + term
-    out[...] = (lat[...].astype(F32) + gate[...] * total).astype(BF16)
+    wide = 512
+    for n in range(out.shape[1] // wide):
+        cols = slice(n * wide, (n + 1) * wide)
+        total = None
+        for t in range(N_TP):
+            term = jnp.dot(
+                o_ref[t], w[t * 256 : (t + 1) * 256, cols], preferred_element_type=F32
+            )
+            total = term if total is None else total + term
+        out[:, cols] = (lat[:, cols].astype(F32) + gate[:, cols] * total).astype(BF16)
 
 
 def run_output(o, w_out, lat, gate):
-    rows, width = lat.shape
-    wide = 512
     return pl.pallas_call(
         output_kernel,
         name="output",
-        grid=(width // wide,),
-        out_shape=jax.ShapeDtypeStruct((rows, width), BF16),
-        in_specs=[
-            pl.BlockSpec((N_TP, rows, 256), lambda n: (0, 0, 0)),
-            pl.BlockSpec((w_out.shape[0], wide), lambda n: (0, n)),
-            pl.BlockSpec((rows, wide), lambda n: (0, n)),
-            pl.BlockSpec((1, wide), lambda n: (0, n)),
-        ],
-        out_specs=pl.BlockSpec((rows, wide), lambda n: (0, n)),
+        out_shape=jax.ShapeDtypeStruct(lat.shape, BF16),
+        in_specs=[VMEM] * 4,
+        out_specs=VMEM,
+        compiler_params=pltpu.CompilerParams(vmem_limit_bytes=12 * 2**20),
     )(o, w_out, lat, gate)
 
 

time: 98.7 us -> 88.6 us (0.90)
  Pallas kernels: 98.3 us -> 85.1 us
  local copies, waits for them, and re-layouts: 0 us -> 3.18 us
    pallas_call x1, Pallas kernels: 83.6 us -> 74.2 us  [run_attention(): pl.pallas_call(attention_kernel, name='attention', out_shape=(jax.ShapeDt...]
    unnamed x0 -> x8, local copies, waits for them, and re-layouts: none -> 3.18 us
    pallas_call x1, Pallas kernels: 5.01 us -> 1.9 us  [run_output(): pl.pallas_call(output_kernel, name='output', out_shape=jax.ShapeDtypeStru...]
    pallas_call x1, Pallas kernels: 8.73 us -> 7.01 us  [run_exchange(): pl.pallas_call(exchange_kernel, name='exchange', out_shape=jax.ShapeDtype...]
where the time goes in v3:
time: 88.6 us; the launch traced here: 88.4 us
  Pallas kernels  85.1 us (96%)
  local copies, waits for them, and re-layouts  3.18 us (4%)
    pallas_call x1, Pallas kernels, run_attention(): pl.pallas_call(attention_kernel, name='attention', out_shape=(jax.ShapeDt...  74.2 us
    pallas_call x1, Pallas kernels, run_exchange(): pl.pallas_call(exchange_kernel, name='exchange', out_shape=jax.ShapeDtype...  7.01 us
    unnamed x8, local copies, waits for them, and re-layouts  3.18 us
    pallas_call x1, Pallas kernels, run_repair(): pl.pallas_call(repair_kernel, name='repair', out_shape=jax.ShapeDtypeStru...  2.01 us
    pallas_call x1, Pallas kernels, run_output(): pl.pallas_call(output_kernel, name='output', out_shape=jax.ShapeDtypeStru...  1.9 us

profile of v3, /device:TPU:0, one launch (start us, length us, event | category | flops | bytes accessed | tf_op | source)
XLA Modules:
  0.0 88.4 jit_solution(2172328155964043172)
XLA Ops:
  0.0 74.2 %attention.1 = (bf16[768,256]{1,0:T(8,128)(2,1)}, f32[8,3072]{1,0:T(8,128)}, bf16[64,3072]{1,0:T(8,128)(2,1)}, bf16[32,384,128]{2,1,0:T(8,128)(2,1)}, bf16[512,128]{1,0:T(8,128)(2,1)}, /*index=5*/f32[1,2048]{1,0:T(1,128)}) custom-call(bf16[192,2048]{1,0:T(8,128)(2,1)} %bitcast.9, bf16[32,2048]{1,0:T(8,128)(2,1)} %bitcast.13, bf16[128,512]{1,0:T(8,128)(2,1)} %ms_hbm.1, ...), custom_call_target="tpu_custom_call" | custom-call | flops 20000000000 | bytes 10000000 | tf_op jit(solution)/shard_map/attention/pallas_call | solution.py:473
  74.2 0.0 copy-start.2
  74.2 0.0 copy-start.3
  74.2 2.0 %repair.1.o_ref = bf16[768,256]{1,0:T(8,128)(2,1)} custom-call(f32[8,3072]{1,0:T(8,128)} %get-tuple-element.11.l_ref, bf16[768,256]{1,0:T(8,128)(2,1)} %get-tuple-element.12.o_in, bf16[64,3072]{1,0:T(8,128)(2,1)} %get-tuple-element.13.q_hbm, bf16[32,384,128]{2,1,0:T(8,128)(2,1)} %get-tuple-element.14.kv_hbm, bf16[512,128]{1,0:T(8,128)(2,1)} %get-tuple-element.15.ctx_hbm, ...), custom_call_target="tpu_custom_call" | custom-call | tf_op jit(solution)/shard_map/repair/pallas_call | solution.py:583
  76.2 0.0 copy-start.1
  76.3 1.0 %copy-done.1 = bf16[768,256]{1,0:T(8,128)(2,1)S(1)} copy-done((bf16[768,256]{1,0:T(8,128)(2,1)S(1)}, bf16[768,256]{1,0:T(8,128)(2,1)}, u32[]{:S(2)}) %copy-start.1) | copy-done | bytes 393240
  77.2 7.0 %exchange.1.o_ref = bf16[4,192,256]{2,1,0:T(8,128)(2,1)S(1)} custom-call(bf16[768,256]{1,0:T(8,128)(2,1)S(1)} %copy-done.1), custom_call_target="tpu_custom_call" | custom-call | bytes 25000000 | tf_op jit(solution)/shard_map/exchange/pallas_call | solution.py:639
  84.3 0.0 copy-done.2
  84.3 0.0 copy-done.3
  84.3 0.0 copy-start
  84.3 2.2 %copy-done = bf16[1024,2048]{1,0:T(8,128)(2,1)S(1)} copy-done((bf16[1024,2048]{1,0:T(8,128)(2,1)S(1)}, bf16[1024,2048]{1,0:T(8,128)(2,1)}, u32[]{:S(2)}) %copy-start) | copy-done | bytes 4194328
  86.5 1.9 %output.1 = bf16[192,2048]{1,0:T(8,128)(2,1)} custom-call(bf16[4,192,256]{2,1,0:T(8,128)(2,1)S(1)} %exchange.1.o_ref, bf16[1024,2048]{1,0:T(8,128)(2,1)S(1)} %copy-done, bf16[192,2048]{1,0:T(8,128)(2,1)S(1)} %bitcast.10, f32[1,2048]{1,0:T(1,128)S(1)} %copy-done.3), custom_call_target="tpu_custom_call" | custom-call | tf_op jit(solution)/shard_map/output/pallas_call | solution.py:667
Async XLA Ops:
  74.2 10.1 %copy-start.2 = (bf16[1,192,2048]{2,1,0:T(8,128)(2,1)S(1)}, bf16[1,192,2048]{2,1,0:T(8,128)(2,1)}, u32[]{:S(2)}) copy-start(bf16[1,192,2048]{2,1,0:T(8,128)(2,1)} %param.16) | copy-start | bytes 2359300
  74.2 10.1 %copy-start.3 = (f32[1,2048]{1,0:T(1,128)S(1)}, f32[1,2048]{1,0:T(1,128)}, u32[]{:S(2)}) copy-start(f32[1,2048]{1,0:T(1,128)} %get-tuple-element.16.gate) | copy-start | bytes 24580
  76.2 1.0 %copy-start.1 = (bf16[768,256]{1,0:T(8,128)(2,1)S(1)}, bf16[768,256]{1,0:T(8,128)(2,1)}, u32[]{:S(2)}) copy-start(bf16[768,256]{1,0:T(8,128)(2,1)} %repair.1.o_ref) | copy-start | bytes 1179652
  84.3 2.2 %copy-start = (bf16[1024,2048]{1,0:T(8,128)(2,1)S(1)}, bf16[1024,2048]{1,0:T(8,128)(2,1)}, u32[]{:S(2)}) copy-start(bf16[1024,2048]{1,0:T(8,128)(2,1)} %w.1) | copy-start | bytes 12582916

commit v4 on v3

--- a/solution.py
+++ b/solution.py
@@ -46,15 +46,17 @@
 VROWS = 80
 FIRST = 5
 UNITS = 32
+RETURNS = [(2, 576, 0, 192), (3, 384, 96, 96), (1, 480, 0, 96), (3, 192, 0, 96), (1, 288, 96, 96)]
 
 
 def attention_kernel(
     lat_hbm, ctx_hbm, ms_hbm, mc_hbm, mg_hbm, wq_hbm, wk_hbm, wv_hbm,
     cond, condc, gain, qg, kg, table, lift,
-    o_out, l_out, q_all, kv_all, ctx_all, gate_out,
+    rows_out, flag_out, o_out, l_out, q_all, kv_all, ctx_all, gate_out,
     xbuf, part, psum_in, mine, full, wall, ubuf, raw, cosb, sinb, scl, sft, cbuf,
     q_out, kvbuf, acc, peak, p_even, p_odd, lat, ctx, m_shift, m_scale, m_gate, wq, wk, wv, load_sem,
     x_send, x_recv, p_send, p_recv, t_send, t_recv, c_send, c_recv, kv_send, kv_recv, keep_sem,
+    obuf, fbuf, flag, o_send, o_recv, f_send, f_recv,
 ):
     sp = lax.axis_index("sp")
     tp = lax.axis_index("tp")
@@ -362,7 +364,7 @@
             ),
         )
         tile = jnp.where(
-            j < 2 * FIRST, 1, jnp.where(j < 16, lax.rem(j, 2), jnp.where(j < 24, 0, 1))
+            j < 2 * FIRST, 1, jnp.where(j < 16, lax.rem(j, 2), jnp.where(j < 24, 1, 0))
         )
         return pair, tile
 
@@ -448,16 +450,56 @@
         work(unit(j + 1), unit(j + 2), p_odd, p_even)
         return carry
 
-    lax.fori_loop(0, (UNITS - 1 - FIRST) // 2, second_step, 0)
-    work((15, 1), None, p_even, None)
-
+    returns = [
+        send(
+            o_out.at[pl.ds(here, count)], obuf.at[tp, pl.ds(there, count)],
+            o_send.at[i], o_recv.at[i], tp_at(k),
+        )
+        for i, (k, here, there, count) in enumerate(RETURNS)
+    ]
+
+    def finish_o(blocks):
+        for g in blocks:
+            at_lanes = pl.ds(g * 512, 512)
+            mean = acc[0:HD, at_lanes] / acc[HD : HD + 1, at_lanes]
+            stack = jnp.concatenate([mean[:, h * 128 : (h + 1) * 128] for h in range(4)], axis=0)
+            o_out[g * 128 : (g + 1) * 128, :] = stack.T.astype(BF16)
+
+    steps = (UNITS - 1 - FIRST) // 2
+    lax.fori_loop(0, steps - 3, second_step, 0)
+    finish_o((3, 4, 5))
+    lax.fori_loop(steps - 3, steps - 2, second_step, 0)
+    for copy, (_, here, _, _) in zip(returns, RETURNS):
+        if here >= 384:
+            copy.start()
+    lax.fori_loop(steps - 2, steps, second_step, 0)
+    work((15, 0), None, p_even, None)
+    finish_o((1, 2))
     l_out[...] = acc[HD : HD + 8, :]
-    for g in range(6):
-        at_lanes = pl.ds(g * 512, 512)
-        mean = acc[0:HD, at_lanes] / acc[HD : HD + 1, at_lanes]
-        stack = jnp.concatenate([mean[:, h * 128 : (h + 1) * 128] for h in range(4)], axis=0)
-        o_out[g * 128 : (g + 1) * 128, :] = stack.T.astype(BF16)
-    for copy in x_copies + p_copies + t_copies + c_copies + kv_copies[0] + kv_copies[1]:
+    peaks = acc[HD : HD + 1, 0:128]
+    for i in range(1, 24):
+        peaks = jnp.maximum(peaks, acc[HD : HD + 1, i * 128 : (i + 1) * 128])
+    flag[...] = jnp.broadcast_to(peaks, (8, 128))
+    fbuf[tp] = flag[...]
+    finish_o((0,))
+    for copy, (_, here, _, _) in zip(returns, RETURNS):
+        if here < 384:
+            copy.start()
+    flags = [
+        send(flag, fbuf.at[tp], f_send.at[k - 1], f_recv.at[k - 1], tp_at(k))
+        for k in range(1, N_TP)
+    ]
+    for copy in flags:
+        copy.start()
+    rows_out[tp] = o_out[0:rows, :]
+    for copy in returns + flags:
+        copy.wait_recv()
+    for k in range(1, N_TP):
+        source = lax.rem(tp + k, N_TP)
+        rows_out[source] = obuf[source]
+    flag_out[...] = fbuf[...]
+    waiting = x_copies + p_copies + t_copies + c_copies + kv_copies[0] + kv_copies[1]
+    for copy in waiting + returns + flags:
         copy.wait_send()
     for s in range(2):
         for slot in range(N_SP):
@@ -474,6 +516,8 @@
         attention_kernel,
         name="attention",
         out_shape=(
+            jax.ShapeDtypeStruct((N_TP, rows, 256), BF16),
+            jax.ShapeDtypeStruct((N_TP, 8, 128), F32),
             jax.ShapeDtypeStruct((768, 256), BF16),
             jax.ShapeDtypeStruct((8, 3072), F32),
             jax.ShapeDtypeStruct((HD, 3072), BF16),
@@ -482,7 +526,7 @@
             jax.ShapeDtypeStruct((1, width), F32),
         ),
         in_specs=[HBM] * 8 + [VMEM] * 6 + [SMEM],
-        out_specs=(VMEM, VMEM, HBM, HBM, HBM, VMEM),
+        out_specs=(VMEM, VMEM, VMEM, VMEM, HBM, HBM, HBM, VMEM),
         scratch_shapes=[
             pltpu.VMEM((3 * rows, width), BF16),
             pltpu.VMEM((24, 128), F32),
@@ -508,9 +552,13 @@
             dma((8,)), dma((8,)), dma((15,)), dma((15,)),
             dma((3,)), dma((3,)), dma((15,)), dma((15,)),
             dma((2 * len(SENDS),)), dma((2 * N_SP,)), dma((2 * N_SP + 2,)),
+            pltpu.VMEM((N_TP, rows, 256), BF16),
+            pltpu.VMEM((N_TP, 8, 128), F32),
+            pltpu.VMEM((8, 128), F32),
+            dma((len(RETURNS),)), dma((len(RETURNS),)), dma((N_TP - 1,)), dma((N_TP - 1,)),
         ],
         compiler_params=pltpu.CompilerParams(
-            collective_id=0, has_side_effects=True, vmem_limit_bytes=60 * 2**20
+            collective_id=0, has_side_effects=True, vmem_limit_bytes=67043328
         ),
         cost_estimate=pl.CostEstimate(
             flops=2 * 10**10, bytes_accessed=10**7, transcendentals=4 * 10**7
@@ -594,14 +642,13 @@
             pltpu.VMEM((1, 512), F32),
             pltpu.SemaphoreType.DMA(()),
         ],
-        compiler_params=pltpu.CompilerParams(vmem_limit_bytes=60 * 2**20),
+        compiler_params=pltpu.CompilerParams(vmem_limit_bytes=67043328),
     )(l, o, q, kv_all, ctx, lift)
 
 
 def exchange_kernel(o_ref, out, obuf, send_sem, recv_sem):
     tp = lax.axis_index("tp")
     rows = o_ref.shape[0] // N_TP
-    half = rows // 2
 
     def tp_at(k):
         return {"tp": lax.rem(tp + k, N_TP)}
@@ -610,10 +657,8 @@
     for k in range(1, N_TP):
         pl.semaphore_signal(barrier, inc=1, device_id=tp_at(k), device_id_type=MESH)
     pl.semaphore_wait(barrier, N_TP - 1)
-    plan = [(2, 576, 0, rows), (3, 192, 0, half), (1, 288, half, half), (3, 384, half, half),
-            (1, 480, 0, half)]
     copies = []
-    for i, (k, here, there, count) in enumerate(plan):
+    for i, (k, here, there, count) in enumerate(RETURNS):
         copies.append(
             pltpu.make_async_remote_copy(
                 src_ref=o_ref.at[pl.ds(here, count)],
@@ -650,15 +695,21 @@
     )(o)
 
 
-def output_kernel(o_ref, w, lat, gate, out):
+def output_kernel(o_ref, w_hbm, lat, gate, out, w, sem):
     wide = 512
-    for n in range(out.shape[1] // wide):
+    count = out.shape[1] // wide
+    loads = [
+        pltpu.make_async_copy(w_hbm.at[:, pl.ds(n * wide, wide)], w.at[n], sem.at[n])
+        for n in range(count)
+    ]
+    for load in loads:
+        load.start()
+    for n in range(count):
         cols = slice(n * wide, (n + 1) * wide)
+        loads[n].wait()
         total = None
         for t in range(N_TP):
-            term = jnp.dot(
-                o_ref[t], w[t * 256 : (t + 1) * 256, cols], preferred_element_type=F32
-            )
+            term = jnp.dot(o_ref[t], w[n, t * 256 : (t + 1) * 256, :], preferred_element_type=F32)
             total = term if total is None else total + term
         out[:, cols] = (lat[:, cols].astype(F32) + gate[:, cols] * total).astype(BF16)
 
@@ -668,9 +719,13 @@
         output_kernel,
         name="output",
         out_shape=jax.ShapeDtypeStruct(lat.shape, BF16),
-        in_specs=[VMEM] * 4,
+        in_specs=[VMEM, HBM, VMEM, VMEM],
         out_specs=VMEM,
-        compiler_params=pltpu.CompilerParams(vmem_limit_bytes=12 * 2**20),
+        scratch_shapes=[
+            pltpu.VMEM((4, w_out.shape[0], w_out.shape[1] // 4), BF16),
+            pltpu.SemaphoreType.DMA((4,)),
+        ],
+        compiler_params=pltpu.CompilerParams(vmem_limit_bytes=67043328),
     )(o, w_out, lat, gate)
 
 
@@ -679,13 +734,21 @@
     w_query, w_key, w_value, q_gain, k_gain, ctx_lift, w_out,
 ):
     lat = latent[0]
-    o, l, q, kv_all, ctx, gate = run_attention(
+    at_owner, flags, o, l, q, kv_all, ctx, gate = run_attention(
         lat, cond, cond_ctx[None, :], context[0], norm_gain.reshape(-1, 128),
         mod_shift, mod_scale, mod_gate, w_query, w_key.T, w_value.T,
         q_gain[None, :], k_gain[None, :], ctx_lift,
     )
-    o = run_repair(l, o, q, kv_all, ctx, ctx_lift)
-    return run_output(run_exchange(o), w_out, lat, gate)[None]
+
+    def again(at_owner, o, l, q, kv_all, ctx):
+        return run_exchange(run_repair(l, o, q, kv_all, ctx, ctx_lift))
+
+    def keep(at_owner, *rest):
+        return at_owner
+
+    safe = jnp.max(flags) < 2.0**100
+    at_owner = lax.cond(safe, keep, again, at_owner, o, l, q, kv_all, ctx)
+    return run_output(at_owner, w_out, lat, gate)[None]
 
 
 def solution(mesh):

time: 88.6 us -> 85.6 us (0.966)
  local copies, waits for them, and re-layouts: 3.18 us -> 0 us
  Pallas kernels: 85.1 us -> 83.2 us
  other arithmetic: 0 us -> 1.33 us
    pallas_call x2 -> x0, Pallas kernels: 9.03 us -> none  [the longest x1 7.01 us: run_exchange(): pl.pallas_call(exchange_kernel, name='exchange', out_shape=jax.ShapeDtype...]
    pallas_call x1, Pallas kernels: 74.2 us -> 78.3 us  [run_attention(): pl.pallas_call(attention_kernel, name='attention', out_shape=(jax.ShapeDt...]
    unnamed x8 -> x0, local copies, waits for them, and re-layouts: 3.18 us -> none
    pallas_call x1, Pallas kernels: 1.9 us -> 4.89 us  [run_output(): pl.pallas_call(output_kernel, name='output', out_shape=jax.ShapeDtypeStru...]
    reduce_max x0 -> x1, other arithmetic: none -> 1.33 us  [on_device(): safe = jnp.max(flags) < 2.0 ** 100]
where the time goes in v4:
time: 85.6 us; the launch traced here: 85.4 us
  Pallas kernels  83.2 us (97%)
  other arithmetic  1.33 us (2%)
    pallas_call x1, Pallas kernels, run_attention(): pl.pallas_call(attention_kernel, name='attention', out_shape=(jax.ShapeDt...  78.3 us
    pallas_call x1, Pallas kernels, run_output(): pl.pallas_call(output_kernel, name='output', out_shape=jax.ShapeDtypeStru...  4.89 us

profile of v4, /device:TPU:0, one launch (start us, length us, event | category | flops | bytes accessed | tf_op | source)
XLA Modules:
  0.0 85.4 jit_solution(13426723548412141753)
XLA Ops:
  0.0 78.3 %attention.1 = (bf16[4,192,256]{2,1,0:T(8,128)(2,1)}, f32[4,8,128]{2,1,0:T(8,128)}, bf16[768,256]{1,0:T(8,128)(2,1)}, f32[8,3072]{1,0:T(8,128)}, bf16[64,3072]{1...) custom-call(bf16[192,2048]{1,0:T(8,128)(2,1)} %bitcast.9, ...), custom_call_target="tpu_custom_call" | custom-call | flops 20000000000 | bytes 10000000 | tf_op jit(solution)/shard_map/attention/pallas_call | solution.py:515
  78.3 1.3 %reduce_max.9 = f32[]{:T(128)} reduce(f32[4,8,128]{2,1,0:T(8,128)} %get-tuple-element.35, f32[]{:T(128)} %constant.1.clone.1), dimensions={0,1,2}, to_apply=%region_0.0 | reduce | flops 4095 | bytes 16392 | tf_op jit(solution)/shard_map/reduce_max | solution.py:749
  80.3 4.9 %output.1 = bf16[192,2048]{1,0:T(8,128)(2,1)} custom-call(bf16[4,192,256]{2,1,0:T(8,128)(2,1)} %get-tuple-element.43.o_ref, bf16[1024,2048]{1,0:T(8,128)(2,1)} %w_hbm.1, bf16[192,2048]{1,0:T(8,128)(2,1)} %bitcast.10, f32[1,2048]{1,0:T(1,128)} %get-tuple-element.42.gate), custom_call_target="tpu_custom_call" | custom-call | tf_op jit(solution)/shard_map/output/pallas_call | solution.py:718
  (1 shorter events, 0.0 us)

commit v5 on v4

--- a/solution.py
+++ b/solution.py
@@ -33,6 +33,10 @@
     return jnp.concatenate([x, jnp.zeros_like(x)], axis=0)
 
 
+PLACES = [
+    (0, 0), (-1, 0), (1, 0), (0, -1), (0, 1), (2, 0), (-1, -1), (-1, 1),
+    (1, -1), (1, 1), (0, 2), (2, -1), (2, 1), (-1, 2), (1, 2), (2, 2),
+]
 SENDS = [
     (0, 1, 1, 0), (0, 2, -1, 0), (0, 3, 0, 1), (0, 4, 0, -1),
     (1, 5, 1, 0), (1, 6, 0, 1), (1, 7, 0, -1),
@@ -41,10 +45,17 @@
     (5, 11, 0, 1), (5, 12, 0, -1),
     (7, 13, 0, -1), (8, 14, 0, 1), (12, 15, 0, -1),
 ]
+MIRROR = [
+    next(i for i, q in enumerate(PLACES) if (q[0] % 4, q[1] % 4) == (p[1] % 4, p[0] % 4))
+    for p in PLACES
+]
+SENDS = [(h, t, dy, dz, 0) for h, t, dy, dz in SENDS] + [
+    (MIRROR[h], MIRROR[t], dz, dy, 1) for h, t, dy, dz in SENDS
+]
 TILE = 1536
 NARROW = 512
 VROWS = 80
-FIRST = 5
+FIRST = 7
 UNITS = 32
 RETURNS = [(2, 576, 0, 192), (3, 384, 96, 96), (1, 480, 0, 96), (3, 192, 0, 96), (1, 288, 96, 96)]
 
@@ -274,17 +285,18 @@
 
     kv_copies = [[], []]
     for s in range(2):
-        for i, (here, there, dy, dz) in enumerate(SENDS):
+        for i, (here, there, dy, dz, part_of) in enumerate(SENDS):
             here, there = here + s * N_SP, there + s * N_SP
+            half_of = pl.ds(192 * part_of, 192)
             kv_copies[s].append(
                 send(
-                    kvbuf.at[here], kvbuf.at[there],
-                    kv_send.at[i + s * len(SENDS)], kv_recv.at[there], near(dy, dz),
+                    kvbuf.at[here, half_of], kvbuf.at[there, half_of],
+                    kv_send.at[i + s * len(SENDS)], kv_recv.at[2 * there + part_of], near(dy, dz),
                 )
             )
 
     def start_from(s, slot):
-        for copy, (here, _, _, _) in zip(kv_copies[s], SENDS):
+        for copy, (here, _, _, _, _) in zip(kv_copies[s], SENDS):
             if here == slot:
                 copy.start()
 
@@ -293,10 +305,9 @@
         return pltpu.make_async_copy(kvbuf.at[slot], kv_all.at[slot], keep_sem.at[slot])
 
     def arrive(s, slot):
-        if slot > 0:
-            next(
-                copy for copy, (_, there, _, _) in zip(kv_copies[s], SENDS) if there == slot
-            ).wait_recv()
+        for copy, (_, there, _, _, _) in zip(kv_copies[s], SENDS):
+            if there == slot:
+                copy.wait_recv()
         start_from(s, slot)
         keep(s, slot).start()
 
@@ -432,8 +443,8 @@
         copy.start()
     work(None, (0, 1), None, p_even)
 
-    events = [(0, 0, (5,)), (1, 0, (6,)), (2, 1, (0, 1)), (3, 0, (7,)), (3, 1, (2, 3)),
-              (4, 1, (4,)), (5, 1, (5,)), (6, 1, (6,)), (8, 1, (7,))]
+    events = [(1, 0, (7,)), (2, 1, (0, 1)), (3, 1, (2,)), (4, 1, (3, 4)), (5, 1, (5,)),
+              (6, 1, (6,)), (7, 1, (7,))]
 
     def second_step(d, carry):
         for when, s, pairs in events:
@@ -497,7 +508,7 @@
     for k in range(1, N_TP):
         source = lax.rem(tp + k, N_TP)
         rows_out[source] = obuf[source]
-    flag_out[...] = fbuf[...]
+    flag_out[0] = (jnp.max(fbuf[...]) < 2.0**100).astype(jnp.int32)
     waiting = x_copies + p_copies + t_copies + c_copies + kv_copies[0] + kv_copies[1]
     for copy in waiting + returns + flags:
         copy.wait_send()
@@ -517,7 +528,7 @@
         name="attention",
         out_shape=(
             jax.ShapeDtypeStruct((N_TP, rows, 256), BF16),
-            jax.ShapeDtypeStruct((N_TP, 8, 128), F32),
+            jax.ShapeDtypeStruct((1,), jnp.int32),
             jax.ShapeDtypeStruct((768, 256), BF16),
             jax.ShapeDtypeStruct((8, 3072), F32),
             jax.ShapeDtypeStruct((HD, 3072), BF16),
@@ -526,7 +537,7 @@
             jax.ShapeDtypeStruct((1, width), F32),
         ),
         in_specs=[HBM] * 8 + [VMEM] * 6 + [SMEM],
-        out_specs=(VMEM, VMEM, VMEM, VMEM, HBM, HBM, HBM, VMEM),
+        out_specs=(VMEM, SMEM, VMEM, VMEM, HBM, HBM, HBM, VMEM),
         scratch_shapes=[
             pltpu.VMEM((3 * rows, width), BF16),
             pltpu.VMEM((24, 128), F32),
@@ -551,7 +562,7 @@
             dma((len(loaded),)),
             dma((8,)), dma((8,)), dma((15,)), dma((15,)),
             dma((3,)), dma((3,)), dma((15,)), dma((15,)),
-            dma((2 * len(SENDS),)), dma((2 * N_SP,)), dma((2 * N_SP + 2,)),
+            dma((2 * len(SENDS),)), dma((4 * N_SP,)), dma((2 * N_SP + 2,)),
             pltpu.VMEM((N_TP, rows, 256), BF16),
             pltpu.VMEM((N_TP, 8, 128), F32),
             pltpu.VMEM((8, 128), F32),
@@ -695,23 +706,29 @@
     )(o)
 
 
-def output_kernel(o_ref, w_hbm, lat, gate, out, w, sem):
-    wide = 512
-    count = out.shape[1] // wide
-    loads = [
-        pltpu.make_async_copy(w_hbm.at[:, pl.ds(n * wide, wide)], w.at[n], sem.at[n])
-        for n in range(count)
-    ]
+def output_kernel(o_hbm, w_hbm, lat_hbm, gate, out, o, w, lat, total, sem):
+    pairs = [(o_hbm, o)]
+    pairs += [(w_hbm.at[pl.ds(t * 256, 256)], w.at[t]) for t in range(N_TP)]
+    pairs += [(lat_hbm, lat)]
+    loads = [pltpu.make_async_copy(a, b, sem.at[i]) for i, (a, b) in enumerate(pairs)]
     for load in loads:
         load.start()
-    for n in range(count):
-        cols = slice(n * wide, (n + 1) * wide)
-        loads[n].wait()
-        total = None
-        for t in range(N_TP):
-            term = jnp.dot(o_ref[t], w[n, t * 256 : (t + 1) * 256, :], preferred_element_type=F32)
-            total = term if total is None else total + term
-        out[:, cols] = (lat[:, cols].astype(F32) + gate[:, cols] * total).astype(BF16)
+    loads[0].wait()
+    wide = 512
+    for t in range(N_TP):
+        loads[1 + t].wait()
+        if t == N_TP - 1:
+            loads[-1].wait()
+        for n in range(out.shape[1] // wide):
+            cols = slice(n * wide, (n + 1) * wide)
+            term = jnp.dot(o[t], w[t, :, cols], preferred_element_type=F32)
+            if t == 0:
+                total[:, cols] = term
+            elif t < N_TP - 1:
+                total[:, cols] += term
+            else:
+                term = total[:, cols] + term
+                out[:, cols] = (lat[:, cols].astype(F32) + gate[:, cols] * term).astype(BF16)
 
 
 def run_output(o, w_out, lat, gate):
@@ -719,11 +736,14 @@
         output_kernel,
         name="output",
         out_shape=jax.ShapeDtypeStruct(lat.shape, BF16),
-        in_specs=[VMEM, HBM, VMEM, VMEM],
+        in_specs=[HBM, HBM, HBM, VMEM],
         out_specs=VMEM,
         scratch_shapes=[
-            pltpu.VMEM((4, w_out.shape[0], w_out.shape[1] // 4), BF16),
-            pltpu.SemaphoreType.DMA((4,)),
+            pltpu.VMEM(o.shape, BF16),
+            pltpu.VMEM((N_TP, 256, w_out.shape[1]), BF16),
+            pltpu.VMEM(lat.shape, BF16),
+            pltpu.VMEM(lat.shape, F32),
+            pltpu.SemaphoreType.DMA((N_TP + 2,)),
         ],
         compiler_params=pltpu.CompilerParams(vmem_limit_bytes=67043328),
     )(o, w_out, lat, gate)
@@ -734,7 +754,7 @@
     w_query, w_key, w_value, q_gain, k_gain, ctx_lift, w_out,
 ):
     lat = latent[0]
-    at_owner, flags, o, l, q, kv_all, ctx, gate = run_attention(
+    at_owner, safe, o, l, q, kv_all, ctx, gate = run_attention(
         lat, cond, cond_ctx[None, :], context[0], norm_gain.reshape(-1, 128),
         mod_shift, mod_scale, mod_gate, w_query, w_key.T, w_value.T,
         q_gain[None, :], k_gain[None, :], ctx_lift,
@@ -746,8 +766,7 @@
     def keep(at_owner, *rest):
         return at_owner
 
-    safe = jnp.max(flags) < 2.0**100
-    at_owner = lax.cond(safe, keep, again, at_owner, o, l, q, kv_all, ctx)
+    at_owner = lax.cond(safe[0] > 0, keep, again, at_owner, o, l, q, kv_all, ctx)
     return run_output(at_owner, w_out, lat, gate)[None]
 
 

time: 85.6 us -> 94.1 us (1.099)
  Pallas kernels: 83.2 us -> 93.1 us
  other arithmetic: 1.33 us -> 0 us
    pallas_call x1, Pallas kernels: 78.3 us -> 88.5 us  [run_attention(): pl.pallas_call(attention_kernel, name='attention', out_shape=(jax.ShapeDt...]
    reduce_max x1 -> x0, other arithmetic: 1.33 us -> none  [on_device(): safe = jnp.max(flags) < 2.0 ** 100]
where the time goes in v5:
time: 94.1 us; the launch traced here: 93.9 us
  Pallas kernels  93.1 us (99%)
    pallas_call x1, Pallas kernels, run_attention(): pl.pallas_call(attention_kernel, name='attention', out_shape=(jax.ShapeDt...  88.5 us
    pallas_call x1, Pallas kernels, run_output(): pl.pallas_call(output_kernel, name='output', out_shape=jax.ShapeDtypeStru...  4.53 us

profile of v5, /device:TPU:0, one launch (start us, length us, event | category | flops | bytes accessed | tf_op | source)
XLA Modules:
  0.0 93.9 jit_solution(5318508450920222313)
XLA Ops:
  0.0 88.5 %attention.1 = (bf16[4,192,256]{2,1,0:T(8,128)(2,1)}, s32[1]{0:T(128)}, bf16[768,256]{1,0:T(8,128)(2,1)}, f32[8,3072]{1,0:T(8,128)}, bf16[64,3072]{1,0:T(8,128)(...) custom-call(bf16[192,2048]{1,0:T(8,128)(2,1)} %bitcast.10, ...), custom_call_target="tpu_custom_call" | custom-call | flops 20000000000 | bytes 10000000 | tf_op jit(solution)/shard_map/attention/pallas_call | solution.py:526
  89.2 4.5 %output.1 = bf16[192,2048]{1,0:T(8,128)(2,1)} custom-call(bf16[4,192,256]{2,1,0:T(8,128)(2,1)} %get-tuple-element.43.o_hbm, bf16[1024,2048]{1,0:T(8,128)(2,1)} %w_hbm.1, bf16[192,2048]{1,0:T(8,128)(2,1)} %bitcast.11, f32[1,2048]{1,0:T(1,128)} %get-tuple-element.42.gate), custom_call_target="tpu_custom_call" | custom-call | tf_op jit(solution)/shard_map/output/pallas_call | solution.py:735
  (1 shorter events, 0.0 us)

commit v6 on v5

--- a/solution.py
+++ b/solution.py
@@ -34,16 +34,16 @@
 
 
 PLACES = [
-    (0, 0), (-1, 0), (1, 0), (0, -1), (0, 1), (2, 0), (-1, -1), (-1, 1),
-    (1, -1), (1, 1), (0, 2), (2, -1), (2, 1), (-1, 2), (1, 2), (2, 2),
+    (0, 0), (-1, 0), (1, 0), (0, -1), (0, 1), (2, 0), (0, 2), (-1, -1),
+    (-1, 1), (1, -1), (1, 1), (2, 1), (1, 2), (2, -1), (-1, 2), (2, 2),
 ]
 SENDS = [
     (0, 1, 1, 0), (0, 2, -1, 0), (0, 3, 0, 1), (0, 4, 0, -1),
-    (1, 5, 1, 0), (1, 6, 0, 1), (1, 7, 0, -1),
-    (2, 8, 0, 1), (2, 9, 0, -1),
-    (3, 10, 0, 1),
-    (5, 11, 0, 1), (5, 12, 0, -1),
-    (7, 13, 0, -1), (8, 14, 0, 1), (12, 15, 0, -1),
+    (1, 5, 1, 0), (1, 7, 0, 1), (1, 8, 0, -1),
+    (2, 9, 0, 1), (2, 10, 0, -1),
+    (3, 6, 0, 1),
+    (5, 11, 0, -1), (5, 13, 0, 1),
+    (8, 14, 0, -1), (9, 12, 0, 1), (11, 15, 0, -1),
 ]
 MIRROR = [
     next(i for i, q in enumerate(PLACES) if (q[0] % 4, q[1] % 4) == (p[1] % 4, p[0] % 4))
@@ -61,13 +61,13 @@
 
 
 def attention_kernel(
-    lat_hbm, ctx_hbm, ms_hbm, mc_hbm, mg_hbm, wq_hbm, wk_hbm, wv_hbm,
+    lat_hbm, ctx_hbm, ms_hbm, mc_hbm, mg_hbm, wq_hbm, wk_hbm, wv_hbm, w_hbm,
     cond, condc, gain, qg, kg, table, lift,
-    rows_out, flag_out, o_out, l_out, q_all, kv_all, ctx_all, gate_out,
+    mixed_out, flag_out, o_out, l_out, q_all, kv_all, ctx_all, gate_out,
     xbuf, part, psum_in, mine, full, wall, ubuf, raw, cosb, sinb, scl, sft, cbuf,
     q_out, kvbuf, acc, peak, p_even, p_odd, lat, ctx, m_shift, m_scale, m_gate, wq, wk, wv, load_sem,
     x_send, x_recv, p_send, p_recv, t_send, t_recv, c_send, c_recv, kv_send, kv_recv, keep_sem,
-    obuf, fbuf, flag, o_send, o_recv, f_send, f_recv,
+    obuf, fbuf, flag, w, w_sem, summed, o_send, o_recv, f_send, f_recv,
 ):
     sp = lax.axis_index("sp")
     tp = lax.axis_index("tp")
@@ -192,6 +192,8 @@
         sine = jnp.sin(angle)
         sinb[g] = jnp.where(even, -sine, sine)
 
+    w_load = pltpu.make_async_copy(w_hbm, w, w_sem)
+    w_load.start()
     for copy in t_copies:
         copy.wait_recv()
 
@@ -367,16 +369,13 @@
                 acc[:, narrow(now[1], n)] += total
 
     def unit(j):
+        i = j - 16
+        late = jnp.where(i < 6, i + 8, jnp.where(i == 6, 8, jnp.where(i < 9, i + 7, i)))
         pair = jnp.where(
-            j < 2 * FIRST,
-            j - FIRST,
-            jnp.where(
-                j < 16, FIRST + (j - 2 * FIRST) // 2, jnp.where(j < 24, j - 8, j - 16)
-            ),
+            j < 2 * FIRST, j - FIRST, jnp.where(j < 16, FIRST + (j - 2 * FIRST) // 2, late)
         )
-        tile = jnp.where(
-            j < 2 * FIRST, 1, jnp.where(j < 16, lax.rem(j, 2), jnp.where(j < 24, 1, 0))
-        )
+        late = jnp.where(i < 6, 1, jnp.where(i == 6, 0, jnp.where(i < 9, 1, 0)))
+        tile = jnp.where(j < 2 * FIRST, 1, jnp.where(j < 16, lax.rem(j, 2), late))
         return pair, tile
 
     c_copies = [
@@ -421,12 +420,13 @@
         work((2 * d + 1, 0), (2 * d + 2, 0), p_odd, p_even)
         return carry
 
-    lax.fori_loop(0, FIRST // 2, first_step, 0)
-    work((FIRST - 1, 0), None, p_even, None)
-
+    lax.fori_loop(0, 1, first_step, 0)
     rc.wait_recv()
     lc.wait_recv()
     project(xbuf, 192, 384)
+    lax.fori_loop(1, FIRST // 2, first_step, 0)
+    work((FIRST - 1, 0), None, p_even, None)
+
     rf.wait_recv()
     lf.wait_recv()
     project(xbuf, 384, 576)
@@ -443,18 +443,16 @@
         copy.start()
     work(None, (0, 1), None, p_even)
 
-    events = [(1, 0, (7,)), (2, 1, (0, 1)), (3, 1, (2,)), (4, 1, (3, 4)), (5, 1, (5,)),
-              (6, 1, (6,)), (7, 1, (7,))]
+    events = [(1, 0, (14, 15)), (1, 1, (1, 2, 3)), (3, 1, (4, 5)), (4, 1, (6, 7, 8, 9)),
+              (5, 1, (10,)), (6, 1, (11, 12)), (7, 1, (13, 14)), (8, 1, (15,))]
 
     def second_step(d, carry):
-        for when, s, pairs in events:
+        for when, s, slots in events:
 
             @pl.when(d == when)
-            def _(s=s, pairs=pairs):
-                for pair in pairs:
-                    for slot in (2 * pair, 2 * pair + 1):
-                        if slot > 0:
-                            arrive(s, slot)
+            def _(s=s, slots=slots):
+                for slot in slots:
+                    arrive(s, slot)
 
         j = FIRST + 2 * d
         work(unit(j), unit(j + 1), p_even, p_odd)
@@ -502,12 +500,25 @@
     ]
     for copy in flags:
         copy.start()
-    rows_out[tp] = o_out[0:rows, :]
+    obuf[tp] = o_out[0:rows, :]
+    w_load.wait()
+    wide = 512
+
+    def heads(source, cols):
+        feature = pl.ds(pl.multiple_of(source * 256, 256), 256)
+        return jnp.dot(obuf[source], w[feature, cols], preferred_element_type=F32)
+
+    for n in range(width // wide):
+        cols = slice(n * wide, (n + 1) * wide)
+        summed[:, cols] = heads(tp, cols)
     for copy in returns + flags:
         copy.wait_recv()
-    for k in range(1, N_TP):
-        source = lax.rem(tp + k, N_TP)
-        rows_out[source] = obuf[source]
+    for n in range(width // wide):
+        cols = slice(n * wide, (n + 1) * wide)
+        others = sum(heads(lax.rem(tp + k, N_TP), cols) for k in range(1, N_TP))
+        mixed_out[:, cols] = (
+            lat[:, cols].astype(F32) + gate_out[:, cols] * (summed[:, cols] + others)
+        ).astype(BF16)
     flag_out[0] = (jnp.max(fbuf[...]) < 2.0**100).astype(jnp.int32)
     waiting = x_copies + p_copies + t_copies + c_copies + kv_copies[0] + kv_copies[1]
     for copy in waiting + returns + flags:
@@ -519,7 +530,7 @@
         copy.wait()
 
 
-def run_attention(lat, cond, condc, ctx, gain, ms, mc, mg, wq, wk, wv, qg, kg, lift):
+def run_attention(lat, cond, condc, ctx, gain, ms, mc, mg, wq, wk, wv, qg, kg, lift, w_out):
     rows, width = lat.shape
     dma = pltpu.SemaphoreType.DMA
     loaded = (lat, ctx, ms, mc, mg, wq, wk, wv)
@@ -527,7 +538,7 @@
         attention_kernel,
         name="attention",
         out_shape=(
-            jax.ShapeDtypeStruct((N_TP, rows, 256), BF16),
+            jax.ShapeDtypeStruct((rows, width), BF16),
             jax.ShapeDtypeStruct((1,), jnp.int32),
             jax.ShapeDtypeStruct((768, 256), BF16),
             jax.ShapeDtypeStruct((8, 3072), F32),
@@ -536,7 +547,7 @@
             jax.ShapeDtypeStruct((512, 128), BF16),
             jax.ShapeDtypeStruct((1, width), F32),
         ),
-        in_specs=[HBM] * 8 + [VMEM] * 6 + [SMEM],
+        in_specs=[HBM] * 9 + [VMEM] * 6 + [SMEM],
         out_specs=(VMEM, SMEM, VMEM, VMEM, HBM, HBM, HBM, VMEM),
         scratch_shapes=[
             pltpu.VMEM((3 * rows, width), BF16),
@@ -566,6 +577,9 @@
             pltpu.VMEM((N_TP, rows, 256), BF16),
             pltpu.VMEM((N_TP, 8, 128), F32),
             pltpu.VMEM((8, 128), F32),
+            pltpu.VMEM(w_out.shape, BF16),
+            dma(()),
+            pltpu.VMEM((rows, width), F32),
             dma((len(RETURNS),)), dma((len(RETURNS),)), dma((N_TP - 1,)), dma((N_TP - 1,)),
         ],
         compiler_params=pltpu.CompilerParams(
@@ -575,7 +589,7 @@
             flops=2 * 10**10, bytes_accessed=10**7, transcendentals=4 * 10**7
         ),
     )(
-        *loaded, cond, condc, gain, qg, kg, jnp.asarray(angle_table()), lift,
+        *loaded, w_out, cond, condc, gain, qg, kg, jnp.asarray(angle_table()), lift,
     )
 
 
@@ -749,25 +763,60 @@
     )(o, w_out, lat, gate)
 
 
+def settle_kernel(mixed, out, buf, sem_in, sem_out):
+    pieces = buf.shape[0]
+    count = buf.shape[1]
+    loads, stores = [], []
+    for i in range(pieces):
+        rows = pl.ds(i * count, count)
+        loads.append(pltpu.make_async_copy(mixed.at[rows], buf.at[i], sem_in.at[i]))
+        stores.append(pltpu.make_async_copy(buf.at[i], out.at[rows], sem_out.at[i]))
+    for load in loads:
+        load.start()
+    for load, store in zip(loads, stores):
+        load.wait()
+        store.start()
+    for store in stores:
+        store.wait()
+
+
+def run_settle(mixed):
+    rows, width = mixed.shape
+    return pl.pallas_call(
+        settle_kernel,
+        name="settle",
+        out_shape=jax.ShapeDtypeStruct(mixed.shape, mixed.dtype),
+        in_specs=[HBM],
+        out_specs=HBM,
+        scratch_shapes=[
+            pltpu.VMEM((4, rows // 4, width), BF16),
+            pltpu.SemaphoreType.DMA((4,)),
+            pltpu.SemaphoreType.DMA((4,)),
+        ],
+        compiler_params=pltpu.CompilerParams(vmem_limit_bytes=67043328),
+    )(mixed)
+
+
 def on_device(
     latent, cond, cond_ctx, context, norm_gain, mod_shift, mod_scale, mod_gate,
     w_query, w_key, w_value, q_gain, k_gain, ctx_lift, w_out,
 ):
     lat = latent[0]
-    at_owner, safe, o, l, q, kv_all, ctx, gate = run_attention(
+    mixed, safe, o, l, q, kv_all, ctx, gate = run_attention(
         lat, cond, cond_ctx[None, :], context[0], norm_gain.reshape(-1, 128),
         mod_shift, mod_scale, mod_gate, w_query, w_key.T, w_value.T,
-        q_gain[None, :], k_gain[None, :], ctx_lift,
+        q_gain[None, :], k_gain[None, :], ctx_lift, w_out,
     )
 
-    def again(at_owner, o, l, q, kv_all, ctx):
-        return run_exchange(run_repair(l, o, q, kv_all, ctx, ctx_lift))
-
-    def keep(at_owner, *rest):
-        return at_owner
-
-    at_owner = lax.cond(safe[0] > 0, keep, again, at_owner, o, l, q, kv_all, ctx)
-    return run_output(at_owner, w_out, lat, gate)[None]
+    def again(mixed, o, l, q, kv_all, ctx):
+        o = run_exchange(run_repair(l, o, q, kv_all, ctx, ctx_lift))
+        return run_output(o, w_out, lat, gate)
+
+    def keep(mixed, *rest):
+        return mixed
+
+    mixed = lax.cond(safe[0] > 0, keep, again, mixed, o, l, q, kv_all, ctx)
+    return run_settle(mixed)[None]
 
 
 def solution(mesh):

time: 94.1 us -> 84.1 us (0.89)
  Pallas kernels: 93.1 us -> 83 us
    pallas_call x1, Pallas kernels: 88.5 us -> 81.1 us  [run_attention(): pl.pallas_call(attention_kernel, name='attention', out_shape=(jax.ShapeDt...]
    pallas_call x1, Pallas kernels: 4.53 us -> 1.96 us  [run_settle(): pl.pallas_call(settle_kernel, name='settle', out_shape=jax.ShapeDtypeStru...]
where the time goes in v6:
time: 84.1 us; the launch traced here: 83.9 us
  Pallas kernels  83 us (99%)
  between operations  0.87 us (1%)
    pallas_call x1, Pallas kernels, run_attention(): pl.pallas_call(attention_kernel, name='attention', out_shape=(jax.ShapeDt...  81.1 us
    pallas_call x1, Pallas kernels, run_settle(): pl.pallas_call(settle_kernel, name='settle', out_shape=jax.ShapeDtypeStru...  1.96 us

profile of v6, /device:TPU:0, one launch (start us, length us, event | category | flops | bytes accessed | tf_op | source)
XLA Modules:
  0.0 83.9 jit_solution(2116844046788750448)
XLA Ops:
  0.0 81.1 %attention.1 = (bf16[192,2048]{1,0:T(8,128)(2,1)}, s32[1]{0:T(128)}, bf16[768,256]{1,0:T(8,128)(2,1)}, f32[8,3072]{1,0:T(8,128)}, bf16[64,3072]{1,0:T(8,128)(2,1...) custom-call(bf16[192,2048]{1,0:T(8,128)(2,1)} %bitcast.10, ...), custom_call_target="tpu_custom_call" | custom-call | flops 20000000000 | bytes 10000000 | tf_op jit(solution)/shard_map/attention/pallas_call | solution.py:537
  81.8 2.0 %settle.1 = bf16[192,2048]{1,0:T(8,128)(2,1)} custom-call(bf16[192,2048]{1,0:T(8,128)(2,1)} %get-tuple-element.52.mixed), custom_call_target="tpu_custom_call" | custom-call | tf_op jit(solution)/shard_map/settle/pallas_call | solution.py:785
  (1 shorter events, 0.0 us)

commit v7 on v6

--- a/solution.py
+++ b/solution.py
@@ -408,23 +408,14 @@
     arrive(0, 1)
     work(None, (0, 0), None, p_even)
 
-    def first_step(d, carry):
-        for pair in range(1, FIRST):
-
-            @pl.when(d == (pair - 1) // 2)
-            def _(pair=pair):
-                arrive(0, 2 * pair)
-                arrive(0, 2 * pair + 1)
-
-        work((2 * d, 0), (2 * d + 1, 0), p_even, p_odd)
-        work((2 * d + 1, 0), (2 * d + 2, 0), p_odd, p_even)
-        return carry
-
-    lax.fori_loop(0, 1, first_step, 0)
-    rc.wait_recv()
-    lc.wait_recv()
-    project(xbuf, 192, 384)
-    lax.fori_loop(1, FIRST // 2, first_step, 0)
+    for j in range(FIRST - 1):
+        arrive(0, 2 * j + 2)
+        arrive(0, 2 * j + 3)
+        work((j, 0), (j + 1, 0), *((p_even, p_odd) if j % 2 == 0 else (p_odd, p_even)))
+        if j == 2:
+            rc.wait_recv()
+            lc.wait_recv()
+            project(xbuf, 192, 384)
     work((FIRST - 1, 0), None, p_even, None)
 
     rf.wait_recv()
@@ -443,8 +434,8 @@
         copy.start()
     work(None, (0, 1), None, p_even)
 
-    events = [(1, 0, (14, 15)), (1, 1, (1, 2, 3)), (3, 1, (4, 5)), (4, 1, (6, 7, 8, 9)),
-              (5, 1, (10,)), (6, 1, (11, 12)), (7, 1, (13, 14)), (8, 1, (15,))]
+    events = [(1, 1, (1, 2, 3)), (2, 0, (14, 15)), (3, 1, (4, 5)), (4, 1, (7, 8, 9)),
+              (5, 1, (6, 10)), (6, 1, (11, 12)), (7, 1, (13, 14)), (8, 1, (15,))]
 
     def second_step(d, carry):
         for when, s, slots in events:

time: 84.1 us -> 84 us (level)
  no operation moved by 1% of the time
where the time goes in v7:
time: 84 us; the launch traced here: 83.8 us
  Pallas kernels  82.9 us (99%)
  between operations  0.87 us (1%)
    pallas_call x1, Pallas kernels, run_attention(): pl.pallas_call(attention_kernel, name='attention', out_shape=(jax.ShapeDt...  81 us
    pallas_call x1, Pallas kernels, run_settle(): pl.pallas_call(settle_kernel, name='settle', out_shape=jax.ShapeDtypeStru...  1.96 us

profile of v7, /device:TPU:0, one launch (start us, length us, event | category | flops | bytes accessed | tf_op | source)
XLA Modules:
  0.0 83.8 jit_solution(6726935961331011825)
XLA Ops:
  0.0 81.0 %attention.1 = (bf16[192,2048]{1,0:T(8,128)(2,1)}, s32[1]{0:T(128)}, bf16[768,256]{1,0:T(8,128)(2,1)}, f32[8,3072]{1,0:T(8,128)}, bf16[64,3072]{1,0:T(8,128)(2,1...) custom-call(bf16[192,2048]{1,0:T(8,128)(2,1)} %bitcast.10, ...), custom_call_target="tpu_custom_call" | custom-call | flops 20000000000 | bytes 10000000 | tf_op jit(solution)/shard_map/attention/pallas_call | solution.py:528
  81.7 2.0 %settle.1 = bf16[192,2048]{1,0:T(8,128)(2,1)} custom-call(bf16[192,2048]{1,0:T(8,128)(2,1)} %get-tuple-element.52.mixed), custom_call_target="tpu_custom_call" | custom-call | tf_op jit(solution)/shard_map/settle/pallas_call | solution.py:776
  (1 shorter events, 0.0 us)

commit v8 on v7

--- a/solution.py
+++ b/solution.py
@@ -55,7 +55,7 @@
 TILE = 1536
 NARROW = 512
 VROWS = 80
-FIRST = 7
+FIRST = 5
 UNITS = 32
 RETURNS = [(2, 576, 0, 192), (3, 384, 96, 96), (1, 480, 0, 96), (3, 192, 0, 96), (1, 288, 96, 96)]
 
@@ -434,8 +434,9 @@
         copy.start()
     work(None, (0, 1), None, p_even)
 
-    events = [(1, 1, (1, 2, 3)), (2, 0, (14, 15)), (3, 1, (4, 5)), (4, 1, (7, 8, 9)),
-              (5, 1, (6, 10)), (6, 1, (11, 12)), (7, 1, (13, 14)), (8, 1, (15,))]
+    events = [(0, 0, (10, 11)), (1, 0, (12, 13)), (1, 1, (1, 2, 3, 4)), (3, 0, (14, 15)),
+              (4, 1, (5, 7, 8)), (5, 1, (6, 9)), (6, 1, (10,)), (7, 1, (11, 12)),
+              (8, 1, (13, 14)), (9, 1, (15,))]
 
     def second_step(d, carry):
         for when, s, slots in events:

time: 84 us -> 80.6 us (0.960)
  Pallas kernels: 82.9 us -> 79.5 us
    pallas_call x1, Pallas kernels: 81 us -> 77.6 us  [run_attention(): pl.pallas_call(attention_kernel, name='attention', out_shape=(jax.ShapeDt...]
where the time goes in v8:
time: 80.6 us; the launch traced here: 80.4 us
  Pallas kernels  79.5 us (99%)
  between operations  0.87 us (1%)
    pallas_call x1, Pallas kernels, run_attention(): pl.pallas_call(attention_kernel, name='attention', out_shape=(jax.ShapeDt...  77.6 us
    pallas_call x1, Pallas kernels, run_settle(): pl.pallas_call(settle_kernel, name='settle', out_shape=jax.ShapeDtypeStru...  1.96 us

profile of v8, /device:TPU:0, one launch (start us, length us, event | category | flops | bytes accessed | tf_op | source)
XLA Modules:
  0.0 80.4 jit_solution(8202814596462503081)
XLA Ops:
  0.0 77.6 %attention.1 = (bf16[192,2048]{1,0:T(8,128)(2,1)}, s32[1]{0:T(128)}, bf16[768,256]{1,0:T(8,128)(2,1)}, f32[8,3072]{1,0:T(8,128)}, bf16[64,3072]{1,0:T(8,128)(2,1...) custom-call(bf16[192,2048]{1,0:T(8,128)(2,1)} %bitcast.10, ...), custom_call_target="tpu_custom_call" | custom-call | flops 20000000000 | bytes 10000000 | tf_op jit(solution)/shard_map/attention/pallas_call | solution.py:529
  78.3 2.0 %settle.1 = bf16[192,2048]{1,0:T(8,128)(2,1)} custom-call(bf16[192,2048]{1,0:T(8,128)(2,1)} %get-tuple-element.52.mixed), custom_call_target="tpu_custom_call" | custom-call | tf_op jit(solution)/shard_map/settle/pallas_call | solution.py:777
  (1 shorter events, 0.0 us)

commit v9 on v8

--- a/solution.py
+++ b/solution.py
@@ -408,15 +408,17 @@
     arrive(0, 1)
     work(None, (0, 0), None, p_even)
 
+    turns = [0, 1, 2, 4, 3]
     for j in range(FIRST - 1):
-        arrive(0, 2 * j + 2)
-        arrive(0, 2 * j + 3)
-        work((j, 0), (j + 1, 0), *((p_even, p_odd) if j % 2 == 0 else (p_odd, p_even)))
-        if j == 2:
+        now, then = turns[j], turns[j + 1]
+        arrive(0, 2 * then)
+        arrive(0, 2 * then + 1)
+        work((now, 0), (then, 0), *((p_even, p_odd) if j % 2 == 0 else (p_odd, p_even)))
+        if j == 1:
             rc.wait_recv()
             lc.wait_recv()
             project(xbuf, 192, 384)
-    work((FIRST - 1, 0), None, p_even, None)
+    work((turns[-1], 0), None, p_even, None)
 
     rf.wait_recv()
     lf.wait_recv()

time: 80.6 us -> 80 us (level)
    pallas_call x1, Pallas kernels: 77.6 us -> 76.7 us  [run_attention(): pl.pallas_call(attention_kernel, name='attention', out_shape=(jax.ShapeDt...]
where the time goes in v9:
time: 80 us; the launch traced here: 79.6 us
  Pallas kernels  78.7 us (98%)
  between operations  0.87 us (1%)
    pallas_call x1, Pallas kernels, run_attention(): pl.pallas_call(attention_kernel, name='attention', out_shape=(jax.ShapeDt...  76.7 us
    pallas_call x1, Pallas kernels, run_settle(): pl.pallas_call(settle_kernel, name='settle', out_shape=jax.ShapeDtypeStru...  1.96 us

profile of v9, /device:TPU:0, one launch (start us, length us, event | category | flops | bytes accessed | tf_op | source)
XLA Modules:
  0.0 79.6 jit_solution(2203589870187149406)
XLA Ops:
  0.0 76.7 %attention.1 = (bf16[192,2048]{1,0:T(8,128)(2,1)}, s32[1]{0:T(128)}, bf16[768,256]{1,0:T(8,128)(2,1)}, f32[8,3072]{1,0:T(8,128)}, bf16[64,3072]{1,0:T(8,128)(2,1...) custom-call(bf16[192,2048]{1,0:T(8,128)(2,1)} %bitcast.10, ...), custom_call_target="tpu_custom_call" | custom-call | flops 20000000000 | bytes 10000000 | tf_op jit(solution)/shard_map/attention/pallas_call | solution.py:531
  77.4 2.0 %settle.1 = bf16[192,2048]{1,0:T(8,128)(2,1)} custom-call(bf16[192,2048]{1,0:T(8,128)(2,1)} %get-tuple-element.52.mixed), custom_call_target="tpu_custom_call" | custom-call | tf_op jit(solution)/shard_map/settle/pallas_call | solution.py:779
  (1 shorter events, 0.0 us)

commit v10 on v9

--- a/solution.py
+++ b/solution.py
@@ -63,11 +63,11 @@
 def attention_kernel(
     lat_hbm, ctx_hbm, ms_hbm, mc_hbm, mg_hbm, wq_hbm, wk_hbm, wv_hbm, w_hbm,
     cond, condc, gain, qg, kg, table, lift,
-    mixed_out, flag_out, o_out, l_out, q_all, kv_all, ctx_all, gate_out,
+    mixed_out, flag_out, o_all, l_all, q_all, kv_all, ctx_all, gate_out,
     xbuf, part, psum_in, mine, full, wall, ubuf, raw, cosb, sinb, scl, sft, cbuf,
     q_out, kvbuf, acc, peak, p_even, p_odd, lat, ctx, m_shift, m_scale, m_gate, wq, wk, wv, load_sem,
     x_send, x_recv, p_send, p_recv, t_send, t_recv, c_send, c_recv, kv_send, kv_recv, keep_sem,
-    obuf, fbuf, flag, w, w_sem, summed, o_send, o_recv, f_send, f_recv,
+    o_out, l_out, obuf, fbuf, flag, w, w_sem, summed, o_send, o_recv, f_send, f_recv,
 ):
     sp = lax.axis_index("sp")
     tp = lax.axis_index("tp")
@@ -494,6 +494,12 @@
     ]
     for copy in flags:
         copy.start()
+    keep_rest += [
+        pltpu.make_async_copy(o_out, o_all, keep_sem.at[2 * N_SP + 2]),
+        pltpu.make_async_copy(l_out, l_all, keep_sem.at[2 * N_SP + 3]),
+    ]
+    for copy in keep_rest[2:]:
+        copy.start()
     obuf[tp] = o_out[0:rows, :]
     w_load.wait()
     wide = 512
@@ -542,7 +548,7 @@
             jax.ShapeDtypeStruct((1, width), F32),
         ),
         in_specs=[HBM] * 9 + [VMEM] * 6 + [SMEM],
-        out_specs=(VMEM, SMEM, VMEM, VMEM, HBM, HBM, HBM, VMEM),
+        out_specs=(VMEM, SMEM, HBM, HBM, HBM, HBM, HBM, VMEM),
         scratch_shapes=[
             pltpu.VMEM((3 * rows, width), BF16),
             pltpu.VMEM((24, 128), F32),
@@ -567,7 +573,9 @@
             dma((len(loaded),)),
             dma((8,)), dma((8,)), dma((15,)), dma((15,)),
             dma((3,)), dma((3,)), dma((15,)), dma((15,)),
-            dma((2 * len(SENDS),)), dma((4 * N_SP,)), dma((2 * N_SP + 2,)),
+            dma((2 * len(SENDS),)), dma((4 * N_SP,)), dma((2 * N_SP + 4,)),
+            pltpu.VMEM((768, 256), BF16),
+            pltpu.VMEM((8, 3072), F32),
             pltpu.VMEM((N_TP, rows, 256), BF16),
             pltpu.VMEM((N_TP, 8, 128), F32),
             pltpu.VMEM((8, 128), F32),

time: 80 us -> 79.8 us (level)
  no operation moved by 1% of the time
where the time goes in v10:
time: 79.8 us; the launch traced here: 79.4 us
  Pallas kernels  78.5 us (98%)
  between operations  0.87 us (1%)
    pallas_call x1, Pallas kernels, run_attention(): pl.pallas_call(attention_kernel, name='attention', out_shape=(jax.ShapeDt...  76.6 us
    pallas_call x1, Pallas kernels, run_settle(): pl.pallas_call(settle_kernel, name='settle', out_shape=jax.ShapeDtypeStru...  1.96 us

profile of v10, /device:TPU:0, one launch (start us, length us, event | category | flops | bytes accessed | tf_op | source)
XLA Modules:
  0.0 79.4 jit_solution(1337001918607107573)
XLA Ops:
  0.0 76.6 %attention.1 = (bf16[192,2048]{1,0:T(8,128)(2,1)}, s32[1]{0:T(128)}, bf16[768,256]{1,0:T(8,128)(2,1)}, f32[8,3072]{1,0:T(8,128)}, bf16[64,3072]{1,0:T(8,128)(2,1...) custom-call(bf16[192,2048]{1,0:T(8,128)(2,1)} %bitcast.10, ...), custom_call_target="tpu_custom_call" | custom-call | flops 20000000000 | bytes 10000000 | tf_op jit(solution)/shard_map/attention/pallas_call | solution.py:537
  77.3 2.0 %settle.1 = bf16[192,2048]{1,0:T(8,128)(2,1)} custom-call(bf16[192,2048]{1,0:T(8,128)(2,1)} %get-tuple-element.52.mixed), custom_call_target="tpu_custom_call" | custom-call | tf_op jit(solution)/shard_map/settle/pallas_call | solution.py:787
  (1 shorter events, 0.0 us)
